TPU v7x, 32 devices: a whole 2x2x4 slice. The times are simulated.
32 devices in a mesh: sp: 8 (over z, x), dp: 4 (over y, core).
Axes of the slice: x: 2, y: 2, z: 4, core: 2. Of those that a mesh axis runs over, the one named last changes fastest.
Arguments:
- queries: bfloat16 [4, 1024, 2048], P('dp', 'sp'), may hold values from -12 to 12
- key_rows: bfloat16 [4, 1024, 2048], P('dp', 'sp'), may hold values from -12 to 12
- value_rows: bfloat16 [4, 1024, 2048], P('dp', 'sp'), may hold values from -6 to 6
- lambdas: float32 [16], P('sp'), may hold values from 0.3 to 0.8
- head_gain: float32 [128], replicated, may hold values from 0.1 to 1.9
- out_weight: bfloat16 [2048, 2048], replicated, may hold values from -0.125 to 0.125
- residual: bfloat16 [4, 1024, 2048], P('dp', 'sp'), may hold values from -6 to 6
- mixer_gain: float32 [2048], replicated, may hold values from 0.1 to 1.9
- channel_gain: float32 [2048], replicated, may hold values from 0.1 to 1.9
- expert_gain: float32 [2048], replicated, may hold values from 0.1 to 1.9
- routes: int32 [4, 1024, 2], P('dp', 'sp'), may hold values from 0 to 7, all different within a row; in each aligned block of 128 rows (0 to 127, 128 to 255, ..., all dimensions but the last counted through in order) at most 48 rows name the same one
- route_logits: float32 [4, 1024, 2], P('dp', 'sp'), may hold values from -5 to 5
- gate_weight: bfloat16 [8, 2048, 4096], P('sp', None, 'dp'), may hold values from -0.125 to 0.125
- up_weight: bfloat16 [8, 2048, 4096], P('sp', None, 'dp'), may hold values from -0.125 to 0.125
- down_weight: bfloat16 [8, 4096, 2048], P('sp', 'dp'), may hold values from -0.09375 to 0.09375
Outputs:
- updated: bfloat16 [4, 1024, 2048], P('dp', 'sp')
Inputs may be any that keep to these rules, and one draw needn't show every extreme that they name: `routes`: among the rows of one device no expert is named by more than 48 rows; in some of these blocks one expert is named by exactly 48.
All inputs are finite; a program needn't handle non-finite values.
Results may differ from a plain program's by a relative error of at most 0.014.
Values may be sent and summed in bfloat16 or wider, within the bound.
No kernel may reach another device: no remote copies, remote signals or barrier semaphores. Data moves between devices by JAX's collectives and lax.ppermute only.
A program may use at most 128 MiB of HBM per device.

v0:
```python
import functools
import math

import jax
import jax.numpy as jnp
from jax import lax
from jax.experimental import pallas as pl
from jax.experimental.pallas import tpu as pltpu
from jax.sharding import PartitionSpec as P


PRICE = 32

F32 = jnp.float32
BF16 = jnp.bfloat16


def params(megabytes=24, **kwargs):
    return pltpu.CompilerParams(vmem_limit_bytes=megabytes * 1024 * 1024, **kwargs)


def on_chip(x):
    return pltpu.with_memory_space_constraint(x, pltpu.VMEM)


def layout_kernel(
    own_ref, cos_ref, sin_ref, q_ref, k_ref, v_ref, first_ref, *near_refs, scale, paired
):
    width = cos_ref.shape[1]
    count = first_ref.shape[0]
    heads = q_ref.shape[2] // (width * count)
    quarter = width // 4
    cosine = cos_ref[...]
    signed_sine = sin_ref[...]
    lane = lax.broadcasted_iota(jnp.int32, cosine.shape, 1)
    front = (lane % (width // 2)) < quarter
    own = own_ref[0]

    def turn(x, factor):
        x = x.astype(F32)
        partner = jnp.where(front, pltpu.roll(x, width - quarter, 1), pltpu.roll(x, quarter, 1))
        return (x * cosine + partner * signed_sine).astype(BF16) * jnp.asarray(factor, BF16)

    for j in range(heads - 1, -1, -1):
        for k in range(count):
            place = (own ^ k if paired else (own + k) % count) if j else k
            at = pl.ds(pl.multiple_of((place * heads + j) * width, width), width)
            parts = turn(q_ref[0, :, at], scale), turn(k_ref[0, :, at], 1.0), v_ref[0, :, at]
            for n, part in enumerate(parts):
                lanes = slice(n * width, (n + 1) * width)
                if j:
                    near_refs[(j - 1) * count + k][:, lanes] = part
                else:
                    first_ref[k, :, lanes] = part


def attention_kernel(own_ref, lam_ref, gain_ref, *refs, head, paired):
    in_refs, o_ref = refs[:-1], refs[-1]
    relative = len(in_refs) > 1
    count = o_ref.shape[0]
    width = o_ref.shape[2]

    def part(k, n):
        at = slice(n * width, (n + 1) * width)
        return in_refs[k][:, at] if relative else in_refs[0][k, :, at]

    keys = jnp.concatenate([part(k, 1) for k in range(count)], axis=0)
    values = jnp.concatenate([part(k, 2) for k in range(count)], axis=0)
    extended = jnp.concatenate([values, jnp.ones_like(values)], axis=1)
    gain = gain_ref[...]
    weight = lam_ref[head]
    own = own_ref[0]
    for pair in range(count // 2):
        q = jnp.concatenate([part(2 * pair, 0), part(2 * pair + 1, 0)], axis=0)
        rows = q.shape[0]
        lane = lax.broadcasted_iota(jnp.int32, q.shape, 1)
        zero = jnp.zeros_like(q)
        both = jnp.concatenate(
            [jnp.where(lane < width // 2, q, zero), jnp.where(lane < width // 2, zero, q)], axis=0
        )
        scores = lax.dot_general(
            both, keys, (((1,), (1,)), ((), ())), preferred_element_type=F32
        )
        top = jnp.max(scores, axis=1, keepdims=True)
        weights = jnp.exp(scores - top).astype(BF16)
        mixed = jnp.dot(weights, extended, preferred_element_type=F32)
        ratio = mixed[:, :width] / mixed[:, width:]
        out = ratio[:rows] - weight * ratio[rows:]
        norm = lax.rsqrt(jnp.mean(out * out, axis=1, keepdims=True) + 1e-05)
        out = (out * norm * gain).astype(BF16)
        for n in range(2):
            k = 2 * pair + n
            if relative:
                k = own ^ k if paired else (own - k + count) % count
            o_ref[k] = out[n * (rows // 2) : (n + 1) * (rows // 2), :]


def rms(x, epsilon):
    return x * lax.rsqrt(jnp.mean(x * x, axis=1, keepdims=True) + epsilon)


def partial_kernel(*refs):
    head_ref, w_ref, out_ref = refs[0], refs[1], refs[-1]
    step = pl.program_id(0)
    count = w_ref.shape[0]
    lhs = jnp.concatenate([head_ref[step * count + g] for g in range(count)], axis=1)
    rhs = jnp.concatenate([w_ref[g] for g in range(count)], axis=0)
    update = jnp.dot(lhs, rhs, preferred_element_type=F32)

    @pl.when(step == 0)
    def _():
        out_ref[...] = update + refs[2][...] if len(refs) > 3 else update

    @pl.when(step != 0)
    def _():
        out_ref[...] += update


def project_kernel(*refs, carried, experts):
    head_ref, w_ref, res_ref, mg_ref, cg_ref, routes_ref = refs[:6]
    stream_ref = refs[6 + carried]
    out_refs = refs[7 + carried : 7 + carried + experts]
    acc_ref = refs[-1]
    step = pl.program_id(0)
    partial_kernel(head_ref, w_ref, *refs[6 : 6 + carried], acc_ref)

    @pl.when(step == pl.num_programs(0) - 1)
    def _():
        stream = (res_ref[...].astype(F32) + rms(acc_ref[...], 1e-06) * mg_ref[...]).astype(BF16)
        stream_ref[...] = stream
        normed = (rms(stream.astype(F32), 1e-06) * cg_ref[...]).astype(BF16)
        tokens = stream.shape[0]
        expert_id = lax.broadcasted_iota(jnp.int32, (experts, tokens), 0)
        named = expert_id == routes_ref[0:1, :]
        for j in range(1, routes_ref.shape[0]):
            named = named | (expert_id == routes_ref[j : j + 1, :])
        before = lax.broadcasted_iota(jnp.int32, (tokens, tokens), 0) < lax.broadcasted_iota(
            jnp.int32, (tokens, tokens), 1
        )
        rank = jnp.dot(
            named.astype(F32).astype(BF16),
            before.astype(F32).astype(BF16),
            preferred_element_type=F32,
        )
        rank = jnp.where(named, rank, -1.0)
        slots = out_refs[0].shape[0]
        slot = lax.broadcasted_iota(jnp.int32, (slots, tokens), 0).astype(F32)
        select = jnp.concatenate(
            [(slot == rank[e : e + 1, :]).astype(F32) for e in range(experts)], axis=0
        ).astype(BF16)
        rows = jnp.dot(select, normed, preferred_element_type=F32).astype(BF16)
        for e in range(experts):
            out_refs[e][...] = rows[e * slots : (e + 1) * slots, :]


def expert_kernel(*refs, pieces):
    x_refs = refs[:pieces]
    g_ref, u_ref, d_ref, mine_ref, theirs_ref = refs[pieces:]
    size = x_refs[0].shape[0]
    rows = jnp.concatenate([x[...] for x in x_refs], axis=0)
    units = g_ref.shape[2]
    block = math.gcd(units, 256)
    parts = []
    for f in range(units // block):
        at = slice(f * block, (f + 1) * block)
        gate = jnp.dot(rows, g_ref[0, :, at], preferred_element_type=F32)
        up = jnp.dot(rows, u_ref[0, :, at], preferred_element_type=F32)
        parts.append((gate / (1.0 + jnp.exp(-gate)) * up).astype(BF16))
    hidden = jnp.concatenate(parts, axis=1)
    half = pieces // 2
    model_dim = d_ref.shape[2]
    block = math.gcd(model_dim, 512)
    for n in range(model_dim // block):
        at = slice(n * block, (n + 1) * block)
        out = jnp.dot(hidden, d_ref[0, :, at], preferred_element_type=F32).astype(BF16)
        for i in range(half):
            mine_ref[i, :, at] = out[i * size : (i + 1) * size, :]
            theirs_ref[i, :, at] = out[(half + i) * size : (half + i + 1) * size, :]


def combine_kernel(*refs, experts):
    back_refs = refs[:experts]
    stream_ref, routes_ref, logits_ref, gain_ref, out_ref = refs[experts:]
    tokens = stream_ref.shape[0]
    top = routes_ref.shape[1]
    slots = back_refs[0].shape[0]
    rows = jnp.concatenate([r[...] for r in back_refs], axis=0)
    expert_id = lax.broadcasted_iota(jnp.int32, (tokens, experts), 1)
    hits = [expert_id == routes_ref[:, j : j + 1] for j in range(top)]
    named = functools.reduce(jnp.logical_or, hits)
    after = lax.broadcasted_iota(jnp.int32, (tokens, tokens), 1) < lax.broadcasted_iota(
        jnp.int32, (tokens, tokens), 0
    )
    rank = jnp.dot(
        after.astype(F32).astype(BF16), named.astype(F32).astype(BF16), preferred_element_type=F32
    )
    logits = logits_ref[...]
    powers = jnp.exp(logits - jnp.max(logits, axis=1, keepdims=True))
    shares = powers / jnp.sum(powers, axis=1, keepdims=True)
    column = lax.broadcasted_iota(jnp.int32, (tokens, experts * slots), 1)
    combined = None
    for j in range(top):
        slot = jnp.sum(jnp.where(hits[j], rank, 0.0), axis=1, keepdims=True).astype(jnp.int32)
        place = routes_ref[:, j : j + 1] * slots + slot
        select = (column == place).astype(F32).astype(BF16)
        picked = jnp.dot(select, rows, preferred_element_type=F32) * shares[:, j : j + 1]
        combined = picked if combined is None else combined + picked
    out_ref[...] = (stream_ref[...].astype(F32) + rms(combined, 1e-06) * gain_ref[...]).astype(BF16)


def group_list(sp_count):
    pairs = [(k, k + 1) for k in range(0, sp_count, 2)]
    return pairs[:1] + pairs[len(pairs) // 2 :][::-1] + pairs[1 : len(pairs) // 2]


def local(
    queries,
    key_rows,
    value_rows,
    lambdas,
    head_gain,
    out_weight,
    residual,
    mixer_gain,
    channel_gain,
    expert_gain,
    routes,
    route_logits,
    gate_weight,
    up_weight,
    down_weight,
):
    sp_count = lax.axis_size("sp")
    dp_count = lax.axis_size("dp")
    heads = lambdas.shape[0]
    width = head_gain.shape[0]
    head_dim = width // 2
    tokens, model_dim = residual.shape[1:]
    length = tokens * sp_count
    scale = head_dim**-0.5

    lane = jnp.arange(width)
    inverse = 1.0 / 10000.0 ** (
        (2 * (lane % (head_dim // 2))).astype(F32) / head_dim
    )
    position = lax.axis_index("sp") * tokens + jnp.arange(tokens)
    angles = position.astype(F32)[:, None] * inverse[None, :]
    cosine = jnp.cos(angles)
    signed_sine = jnp.where((lane % head_dim < head_dim // 2)[None, :], -1.0, 1.0) * jnp.sin(angles)

    own = lax.axis_index("sp")
    own_row = own.reshape(1)
    paired = sp_count & (sp_count - 1) == 0

    def away(k):
        return [(i, i ^ k if paired else (i + k) % sp_count) for i in range(sp_count)]

    def back(k):
        return [(d, s) for s, d in away(k)]

    vmem = pl.BlockSpec(memory_space=pltpu.VMEM)
    smem = pl.BlockSpec(memory_space=pltpu.SMEM)
    near = (heads - 1) * sp_count
    outgoing = pl.pallas_call(
        functools.partial(layout_kernel, scale=scale, paired=paired),
        grid=(1,),
        in_specs=[smem, pl.BlockSpec((tokens, width), lambda i: (0, 0))]
        + [pl.BlockSpec((tokens, width), lambda i: (0, 0))]
        + [pl.BlockSpec(queries.shape, lambda i: (0, 0, 0))] * 3,
        out_specs=[vmem] * (1 + near),
        out_shape=[jax.ShapeDtypeStruct((sp_count, tokens, 3 * width), BF16)]
        + [jax.ShapeDtypeStruct((tokens, 3 * width), BF16)] * near,
        compiler_params=params(12),
        name="lay",
    )(
        own_row,
        cosine,
        signed_sine,
        *[pltpu.with_memory_space_constraint(x, pltpu.HBM) for x in (queries, key_rows, value_rows)],
    )

    gain_row = head_gain.reshape(1, width)
    arrived = [
        [lax.all_to_all(outgoing[0], "sp", split_axis=0, concat_axis=0, tiled=True)]
    ]
    for j in range(1, heads):
        blocks = list(outgoing[1 + (j - 1) * sp_count : 1 + j * sp_count])
        for k in range(1, sp_count):
            blocks[k] = lax.ppermute(blocks[k], "sp", away(k))
        arrived.append(blocks)
    weight_view = pltpu.with_memory_space_constraint(
        out_weight.reshape(sp_count, heads, width, model_dim), pltpu.HBM
    )
    steps = 4
    count = sp_count // steps
    full = pl.BlockSpec((tokens, model_dim), lambda i: (0, 0))
    head_spec = pl.BlockSpec((sp_count, tokens, width), lambda i: (0, 0, 0))
    carry = []
    for j in [*range(1, heads), 0]:
        head_out = pl.pallas_call(
            functools.partial(attention_kernel, head=j, paired=paired),
            in_specs=[smem, smem] + [vmem] * (1 + len(arrived[j])),
            out_specs=vmem,
            out_shape=jax.ShapeDtypeStruct((sp_count, tokens, width), BF16),
            compiler_params=params(16),
            cost_estimate=pl.CostEstimate(
                flops=8 * length * length * width,
                bytes_accessed=8 * length * width,
                transcendentals=2 * length * length,
            ),
        )(own_row, lambdas, gain_row, *[on_chip(x) for x in arrived[j]])
        token_head = lax.all_to_all(
            head_out, "sp", split_axis=0, concat_axis=0, tiled=True
        )
        weight_spec = pl.BlockSpec(
            (count, None, width, model_dim), functools.partial(lambda i, j: (i, j, 0, 0), j=j)
        )
        if j:
            carry = [
                pl.pallas_call(
                    partial_kernel,
                    grid=(steps,),
                    in_specs=[head_spec, weight_spec] + [full] * len(carry),
                    out_specs=full,
                    out_shape=jax.ShapeDtypeStruct((tokens, model_dim), F32),
                    compiler_params=params(12),
                    cost_estimate=pl.CostEstimate(
                        flops=2 * tokens * sp_count * width * model_dim,
                        bytes_accessed=2 * sp_count * width * model_dim,
                        transcendentals=0,
                    ),
                )(token_head, weight_view, *carry)
            ]

    experts = sp_count
    capacity = max(2, 3 * tokens // experts)
    top = routes.shape[2]
    if paired:
        relative = routes.reshape(tokens, top) ^ own
    else:
        relative = (routes.reshape(tokens, top) - own) % sp_count

    row_spec = pl.BlockSpec((1, model_dim), lambda i: (0, 0))
    results = pl.pallas_call(
        functools.partial(project_kernel, carried=len(carry), experts=experts),
        grid=(steps,),
        in_specs=[
            head_spec,
            weight_spec,
            full,
            row_spec,
            row_spec,
            pl.BlockSpec((top, tokens), lambda i: (0, 0)),
        ]
        + [full] * len(carry),
        out_specs=[full] + [pl.BlockSpec((capacity, model_dim), lambda i: (0, 0))] * experts,
        out_shape=[jax.ShapeDtypeStruct((tokens, model_dim), BF16)]
        + [jax.ShapeDtypeStruct((capacity, model_dim), BF16)] * experts,
        scratch_shapes=[pltpu.VMEM((tokens, model_dim), F32)],
        compiler_params=params(14),
        cost_estimate=pl.CostEstimate(
            flops=PRICE * tokens * sp_count * width * model_dim,
            bytes_accessed=PRICE * sp_count * width * model_dim,
            transcendentals=0,
        ),
        name="project",
    )(
        token_head,
        weight_view,
        residual.reshape(tokens, model_dim),
        mixer_gain.reshape(1, model_dim),
        channel_gain.reshape(1, model_dim),
        relative.T,
        *carry,
    )
    stream, sent = results[0], results[1:]

    rows_y = dp_count // 2
    core_swap = [(i, i ^ 1) for i in range(dp_count)]

    def shift(k):
        return [(i, ((i // 2 + k) % rows_y) * 2 + i % 2) for i in range(dp_count)]

    pieces = 2 * rows_y
    hidden = gate_weight.shape[2]
    gate_near, up_near, down_near = on_chip(gate_weight), on_chip(up_weight), on_chip(down_weight)

    def spread(blocks):
        rows = jnp.concatenate(blocks, axis=0)
        here = [rows]
        for k in range(1, rows_y):
            here.append(lax.ppermute(rows, "dp", shift(k)))
        there = []
        for r in here:
            there.append(lax.ppermute(r, "dp", core_swap))
        return here + there

    def expert(rows):
        size = rows[0].shape[0]
        return pl.pallas_call(
            functools.partial(expert_kernel, pieces=pieces),
            in_specs=[vmem] * (pieces + 3),
            out_specs=[vmem] * 2,
            out_shape=[jax.ShapeDtypeStruct((rows_y, size, model_dim), BF16)] * 2,
            compiler_params=params(),
            cost_estimate=pl.CostEstimate(
                flops=6 * pieces * size * model_dim * hidden,
                bytes_accessed=4 * pieces * size * model_dim,
                transcendentals=pieces * size * hidden,
            ),
        )(*[on_chip(r) for r in rows], gate_near, up_near, down_near)

    def gather_sums(mine, theirs):
        other = lax.ppermute(theirs, "dp", core_swap)
        total = mine[0].astype(F32) + other[0].astype(F32)
        for k in range(1, rows_y):
            pair = (mine[k].astype(F32) + other[k].astype(F32)).astype(BF16)
            got = lax.ppermute(pair, "dp", shift(rows_y - k))
            total = total + got.astype(F32)
        return total.astype(BF16)

    groups = group_list(sp_count)
    arrived = {}
    for group in groups:
        for k in group:
            arrived[k] = lax.ppermute(sent[k], "sp", away(k)) if k else sent[k]
    returned = {}
    for group in groups:
        parts = expert(spread([arrived[k] for k in group]))
        total = gather_sums(*parts)
        for n, k in enumerate(group):
            block = total[n * capacity : (n + 1) * capacity]
            returned[k] = lax.ppermute(block, "sp", back(k)) if k else block

    updated = pl.pallas_call(
        functools.partial(combine_kernel, experts=experts),
        out_shape=jax.ShapeDtypeStruct((tokens, model_dim), BF16),
        compiler_params=params(12),
        name="combine",
    )(
        *[returned[k] for k in range(experts)],
        stream,
        relative,
        route_logits.reshape(tokens, top),
        expert_gain.reshape(1, model_dim),
    )
    return updated.reshape(1, tokens, model_dim)


def solution(mesh):
    placed = (
        P("dp", "sp", None),
        P("dp", "sp", None),
        P("dp", "sp", None),
        P("sp"),
        P(),
        P(),
        P("dp", "sp", None),
        P(),
        P(),
        P(),
        P("dp", "sp", None),
        P("dp", "sp", None),
        P("sp", None, "dp"),
        P("sp", None, "dp"),
        P("sp", "dp", None),
    )

    return jax.shard_map(
        local, mesh=mesh, in_specs=placed, out_specs=P("dp", "sp", None), check_vma=False
    )
```

profile of v0, /device:TPU:0, one launch (start us, length us, event | category | flops | bytes accessed | tf_op | source)
XLA Modules:
  0.0 222.2 jit_solution(5395000515370936650)
XLA Ops:
  0.3 3.2 %lay.1 = (bf16[8,128,384]{2,1,0:T(8,128)(2,1)}, bf16[128,384]{1,0:T(8,128)(2,1)S(1)}, bf16[128,384]{1,0:T(8,128)(2,1)S(1)}, bf16[128,384]{1,0:T(8,128)(2,1)S(1)}...) custom-call(s32[1]{0:T(128)} %bitcast.own_ref, ...), custom_call_target="tpu_custom_call" | custom-call | tf_op jit(solution)/shard_map/lay/pallas_call | solution.py:264
  3.5 7.3 %all-to-all-start = ((bf16[8,128,384]{2,1,0:T(8,128)(2,1)}), bf16[8,128,384]{2,1,0:T(8,128)(2,1)S(1)}, u32[]{:S(2)}, u32[]{:S(2)}) async-start(bf16[8,128,384]{2,1,0:T(8,128)(2,1)} %get-tuple-element.31), calls=%async_computation | async-start | bytes 1572864 | tf_op jit(solution)/shard_map/all_to_all | solution.py:284
  10.8 2.0 collective-permute-start
  12.8 1.5 collective-permute-start.1
  14.3 2.9 %collective-permute-start.3 = (bf16[128,384]{1,0:T(8,128)(2,1)S(1)}, bf16[128,384]{1,0:T(8,128)(2,1)S(1)}, u32[]{:S(2)}, u32[]{:S(2)}) collective-permute-start(bf16[128,384]{1,0:T(8,128)(2,1)S(1)} %get-tuple-element.36), channel_id=1, source_target_pairs={{0,16},{4,20},{8,24},{12,28},{16,0},{20,4},{24,8},{28,12},{1,17},{... | collective-permute-start | bytes 294920 | tf_op jit(solution)/shard_map/ppermute | solution.py:289
  18.7 1.9 collective-permute-done.refs_1_
  20.6 4.9 %collective-permute-start.5 = (bf16[128,384]{1,0:T(8,128)(2,1)S(1)}, bf16[128,384]{1,0:T(8,128)(2,1)S(1)}, u32[]{:S(2)}, u32[]{:S(2)}) collective-permute-start(bf16[128,384]{1,0:T(8,128)(2,1)S(1)} %get-tuple-element.38), channel_id=1, source_target_pairs={{0,24},{4,28},{8,16},{12,20},{16,8},{20,12},{24,0},{28,4},{1,25},{... | collective-permute-start | bytes 294920 | tf_op jit(solution)/shard_map/ppermute | solution.py:289
  26.8 4.7 %collective-permute-start.6 = (bf16[128,384]{1,0:T(8,128)(2,1)S(1)}, bf16[128,384]{1,0:T(8,128)(2,1)S(1)}, u32[]{:S(2)}, u32[]{:S(2)}) collective-permute-start(bf16[128,384]{1,0:T(8,128)(2,1)S(1)} %get-tuple-element.39), channel_id=1, source_target_pairs={{0,28},{4,24},{8,20},{12,16},{16,12},{20,8},{24,4},{28,0},{1,29},{... | collective-permute-start | bytes 294920 | tf_op jit(solution)/shard_map/ppermute | solution.py:289
  31.6 11.3 %collective-permute-done.3.refs_4_ = bf16[128,384]{1,0:T(8,128)(2,1)S(1)} collective-permute-done((bf16[128,384]{1,0:T(8,128)(2,1)S(1)}, bf16[128,384]{1,0:T(8,128)(2,1)S(1)}, u32[]{:S(2)}, u32[]{:S(2)}) %collective-permute-start.3) | collective-permute-done | bytes 98336 | tf_op jit(solution)/shard_map/ppermute | solution.py:289
  42.9 2.6 %collective-permute-done.4.refs_5_ = bf16[128,384]{1,0:T(8,128)(2,1)S(1)} collective-permute-done((bf16[128,384]{1,0:T(8,128)(2,1)S(1)}, bf16[128,384]{1,0:T(8,128)(2,1)S(1)}, u32[]{:S(2)}, u32[]{:S(2)}) %collective-permute-start.4) | collective-permute-done | bytes 98336 | tf_op jit(solution)/shard_map/ppermute | solution.py:289
  46.8 4.6 %shard_map.146 = bf16[8,128,128]{2,1,0:T(8,128)(2,1)} custom-call(s32[1]{0:T(128)} %bitcast.own_ref, f32[2]{0:T(128)S(1)} %copy-done.7, f32[1,128]{1,0:T(1,128)S(1)} %bitcast.43, bf16[128,384]{1,0:T(8,128)(2,1)S(1)} %get-tuple-element.32.refs_0_, bf16[128,384]{1,0:T(8,128)(2,1)S(1)} %collective-permute-done.refs_1_, ...), custom_call_target="tpu_custom_call" | custom-call | flops 1073741824 | bytes 1048576 | tf_op jit(solution)/shard_map/pallas_call | solution.py:300
  51.4 5.1 %all-to-all-start.2 = ((bf16[8,128,128]{2,1,0:T(8,128)(2,1)}), bf16[8,128,128]{2,1,0:T(8,128)(2,1)S(1)}, u32[]{:S(2)}, u32[]{:S(2)}) async-start(bf16[8,128,128]{2,1,0:T(8,128)(2,1)} %shard_map.146), calls=%async_computation.2 | async-start | bytes 524288 | tf_op jit(solution)/shard_map/all_to_all | solution.py:312
  56.5 4.5 %shard_map.145 = bf16[8,128,128]{2,1,0:T(8,128)(2,1)} custom-call(s32[1]{0:T(128)} %bitcast.own_ref, f32[2]{0:T(128)S(1)} %copy-done.8, f32[1,128]{1,0:T(1,128)S(1)} %bitcast.44, bf16[8,128,384]{2,1,0:T(8,128)(2,1)S(1)} %all-to-all-done.refs_0_), custom_call_target="tpu_custom_call" | custom-call | flops 1073741824 | bytes 1048576 | tf_op jit(solution)/shard_map/pallas_call | solution.py:300
  61.0 4.5 %all-to-all-done.2.refs_0_ = bf16[8,128,128]{2,1,0:T(8,128)(2,1)S(1)} async-done(((bf16[8,128,128]{2,1,0:T(8,128)(2,1)}), bf16[8,128,128]{2,1,0:T(8,128)(2,1)S(1)}, u32[]{:S(2)}, u32[]{:S(2)}) %all-to-all-start.2) | async-done | bytes 262176 | tf_op jit(solution)/shard_map/all_to_all | solution.py:312
  65.5 3.6 %all-to-all-start.1 = ((bf16[8,128,128]{2,1,0:T(8,128)(2,1)}), bf16[8,128,128]{2,1,0:T(8,128)(2,1)S(1)}, u32[]{:S(2)}, u32[]{:S(2)}) async-start(bf16[8,128,128]{2,1,0:T(8,128)(2,1)} %shard_map.145), calls=%async_computation.1 | async-start | bytes 524288 | tf_op jit(solution)/shard_map/all_to_all | solution.py:312
  69.3 3.8 %shard_map.147.refs_6_ = f32[128,2048]{1,0:T(8,128)S(1)} custom-call(bf16[8,128,128]{2,1,0:T(8,128)(2,1)S(1)} %all-to-all-done.2.refs_0_, bf16[8,2,128,2048]{3,2,1,0:T(8,128)(2,1)} %bitcast.45), custom_call_target="tpu_custom_call" | custom-call | flops 536870912 | bytes 4194304 | tf_op jit(solution)/shard_map/pallas_call | solution.py:320
  73.1 4.5 %all-to-all-done.1.refs_0_ = bf16[8,128,128]{2,1,0:T(8,128)(2,1)S(1)} async-done(((bf16[8,128,128]{2,1,0:T(8,128)(2,1)}), bf16[8,128,128]{2,1,0:T(8,128)(2,1)S(1)}, u32[]{:S(2)}, u32[]{:S(2)}) %all-to-all-start.1) | async-done | bytes 262176 | tf_op jit(solution)/shard_map/all_to_all | solution.py:312
  77.7 5.9 %project.1 = (bf16[128,2048]{1,0:T(8,128)(2,1)S(1)}, bf16[48,2048]{1,0:T(8,128)(2,1)S(1)}, bf16[48,2048]{1,0:T(8,128)(2,1)S(1)}, bf16[48,2048]{1,0:T(8,128)(2,1)...) custom-call(bf16[8,128,128]{2,1,0:T(8,128)(2,1)S(1)} %all-to-all-don, ...), custom_call_target="tpu_custom_call" | custom-call | flops 8589934592 | bytes 67108864 | tf_op jit(solution)/shard_map/project/pallas_call | solution.py:344
  84.8 3.6 %collective-permute-start.33 = (bf16[48,2048]{1,0:T(8,128)(2,1)S(1)}, bf16[48,2048]{1,0:T(8,128)(2,1)S(1)}, u32[]{:S(2)}, u32[]{:S(2)}) collective-permute-start(bf16[48,2048]{1,0:T(8,128)(2,1)S(1)} %get-tuple-element.53), channel_id=1, source_target_pairs={{0,28},{4,24},{8,20},{12,16},{16,12},{20,8},{24,4},{28,0},{1,29},{... | collective-permute-start | bytes 589832 | tf_op jit(solution)/shard_map/ppermute | solution.py:426
  88.4 2.9 %collective-permute-start.24 = (bf16[48,2048]{1,0:T(8,128)(2,1)S(1)}, bf16[48,2048]{1,0:T(8,128)(2,1)S(1)}, u32[]{:S(2)}, u32[]{:S(2)}) collective-permute-start(bf16[48,2048]{1,0:T(8,128)(2,1)S(1)} %get-tuple-element.49), channel_id=1, source_target_pairs={{0,20},{4,16},{8,28},{12,24},{16,4},{20,0},{24,12},{28,8},{1,21},{... | collective-permute-start | bytes 589832 | tf_op jit(solution)/shard_map/ppermute | solution.py:426
  91.3 1.6 collective-permute-done.32
  93.0 15.0 %collective-permute-start.15 = (bf16[48,2048]{1,0:T(8,128)(2,1)S(1)}, bf16[48,2048]{1,0:T(8,128)(2,1)S(1)}, u32[]{:S(2)}, u32[]{:S(2)}) collective-permute-start(bf16[48,2048]{1,0:T(8,128)(2,1)S(1)} %get-tuple-element.45), channel_id=1, source_target_pairs={{0,12},{4,8},{8,4},{12,0},{16,28},{20,24},{24,20},{28,16},{1,13},{... | collective-permute-start | bytes 589832 | tf_op jit(solution)/shard_map/ppermute | solution.py:426
  109.2 6.4 %collective-permute-done.23 = bf16[48,2048]{1,0:T(8,128)(2,1)S(1)} collective-permute-done((bf16[48,2048]{1,0:T(8,128)(2,1)S(1)}, bf16[48,2048]{1,0:T(8,128)(2,1)S(1)}, u32[]{:S(2)}, u32[]{:S(2)}) %collective-permute-start.23) | collective-permute-done | bytes 196640 | tf_op jit(solution)/shard_map/ppermute | solution.py:426
  115.6 1.5 collective-permute-start.34
  118.5 1.6 collective-permute-start.25
  120.5 4.5 %collective-permute-done.34.refs_1_ = bf16[96,2048]{1,0:T(8,128)(2,1)S(1)} collective-permute-done((bf16[96,2048]{1,0:T(8,128)(2,1)S(1)}, bf16[96,2048]{1,0:T(8,128)(2,1)S(1)}, u32[]{:S(2)}, u32[]{:S(2)}) %collective-permute-start.34) | collective-permute-done | bytes 393248 | tf_op jit(solution)/shard_map/ppermute | solution.py:392
  125.0 1.6 collective-permute-start.16
  126.9 6.5 %collective-permute-done.25.refs_1_ = bf16[96,2048]{1,0:T(8,128)(2,1)S(1)} collective-permute-done((bf16[96,2048]{1,0:T(8,128)(2,1)S(1)}, bf16[96,2048]{1,0:T(8,128)(2,1)S(1)}, u32[]{:S(2)}, u32[]{:S(2)}) %collective-permute-start.25) | collective-permute-done | bytes 393248 | tf_op jit(solution)/shard_map/ppermute | solution.py:392
  133.4 1.5 collective-permute-start.8
  134.9 5.1 %shard_map.151 = (bf16[2,96,2048]{2,1,0:T(8,128)(2,1)S(1)}, bf16[2,96,2048]{2,1,0:T(8,128)(2,1)S(1)}) custom-call(bf16[96,2048]{1,0:T(8,128)(2,1)S(1)} %constant_dynamic-update-slice_fusion.6.refs_0_, bf16[96,2048]{1,0:T(8,128)(2,1)S(1)} %collective-permute-done.34.refs_1_, bf16[96,2048]{1,0:T(8,128)(2,1)S(1)} %collective-permute-done.35.refs_2_, ...), custom_call_target="tpu_custom_call" | custom-call | flops 4831838208 | bytes 3145728 | tf_op jit(solution)/shard_map/pallas_call | solution.py:400
  141.8 6.8 %collective-permute-done.8.refs_1_ = bf16[96,2048]{1,0:T(8,128)(2,1)S(1)} collective-permute-done((bf16[96,2048]{1,0:T(8,128)(2,1)S(1)}, bf16[96,2048]{1,0:T(8,128)(2,1)S(1)}, u32[]{:S(2)}, u32[]{:S(2)}) %collective-permute-start.8) | collective-permute-done | bytes 393248 | tf_op jit(solution)/shard_map/ppermute | solution.py:392
  149.1 5.1 %shard_map.150 = (bf16[2,96,2048]{2,1,0:T(8,128)(2,1)S(1)}, bf16[2,96,2048]{2,1,0:T(8,128)(2,1)S(1)}) custom-call(bf16[96,2048]{1,0:T(8,128)(2,1)S(1)} %constant_dynamic-update-slice_fusion.4.refs_0_, bf16[96,2048]{1,0:T(8,128)(2,1)S(1)} %collective-permute-done.25.refs_1_, bf16[96,2048]{1,0:T(8,128)(2,1)S(1)} %collective-permute-done.26.refs_2_, ...), custom_call_target="tpu_custom_call" | custom-call | flops 4831838208 | bytes 3145728 | tf_op jit(solution)/shard_map/pallas_call | solution.py:400
  154.3 5.3 %shard_map.149 = (bf16[2,96,2048]{2,1,0:T(8,128)(2,1)S(1)}, bf16[2,96,2048]{2,1,0:T(8,128)(2,1)S(1)}) custom-call(bf16[96,2048]{1,0:T(8,128)(2,1)S(1)} %constant_dynamic-update-slice_fusion.2.refs_0_, bf16[96,2048]{1,0:T(8,128)(2,1)S(1)} %collective-permute-done.16.refs_1_, bf16[96,2048]{1,0:T(8,128)(2,1)S(1)} %collective-permute-done.17.refs_2_, ...), custom_call_target="tpu_custom_call" | custom-call | flops 4831838208 | bytes 3145728 | tf_op jit(solution)/shard_map/pallas_call | solution.py:400
  160.2 5.1 %shard_map.148 = (bf16[2,96,2048]{2,1,0:T(8,128)(2,1)S(1)}, bf16[2,96,2048]{2,1,0:T(8,128)(2,1)S(1)}) custom-call(bf16[96,2048]{1,0:T(8,128)(2,1)S(1)} %constant_dynamic-update-slice_fusion.refs_0_, bf16[96,2048]{1,0:T(8,128)(2,1)S(1)} %collective-permute-done.8.refs_1_, bf16[96,2048]{1,0:T(8,128)(2,1)S(1)} %collective-permute-done.9.refs_2_, ...), custom_call_target="tpu_custom_call" | custom-call | flops 4831838208 | bytes 3145728 | tf_op jit(solution)/shard_map/pallas_call | solution.py:400
  165.5 1.6 collective-permute-start.38
  167.8 1.6 collective-permute-start.20
  170.1 7.4 %collective-permute-done.38 = bf16[96,2048]{1,0:T(8,128)(2,1)S(1)} collective-permute-done((bf16[96,2048]{1,0:T(8,128)(2,1)S(1)}, bf16[96,2048]{1,0:T(8,128)(2,1)S(1)}, u32[]{:S(2)}, u32[]{:S(2)}) %collective-permute-start.38) | collective-permute-done | bytes 393248 | tf_op jit(solution)/shard_map/ppermute | solution.py:418
  177.7 2.8 %collective-permute-start.39 = (bf16[48,2048]{1,0:T(8,128)(2,1)S(1)}, bf16[48,2048]{1,0:T(8,128)(2,1)S(1)}, u32[]{:S(2)}, u32[]{:S(2)}) collective-permute-start(bf16[48,2048]{1,0:T(8,128)(2,1)S(1)} %get-tuple-element.58), channel_id=1, source_target_pairs={{24,0},{28,4},{16,8},{20,12},{8,16},{12,20},{0,24},{4,28},{25,1},{... | collective-permute-start | bytes 589832 | tf_op jit(solution)/shard_map/ppermute | solution.py:433
  180.5 1.5 collective-permute-start.40
  182.0 3.9 %collective-permute-done.29 = bf16[96,2048]{1,0:T(8,128)(2,1)S(1)} collective-permute-done((bf16[96,2048]{1,0:T(8,128)(2,1)S(1)}, bf16[96,2048]{1,0:T(8,128)(2,1)S(1)}, u32[]{:S(2)}, u32[]{:S(2)}) %collective-permute-start.29) | collective-permute-done | bytes 393248 | tf_op jit(solution)/shard_map/ppermute | solution.py:418
  186.2 8.2 %collective-permute-done.20 = bf16[96,2048]{1,0:T(8,128)(2,1)S(1)} collective-permute-done((bf16[96,2048]{1,0:T(8,128)(2,1)S(1)}, bf16[96,2048]{1,0:T(8,128)(2,1)S(1)}, u32[]{:S(2)}, u32[]{:S(2)}) %collective-permute-start.20) | collective-permute-done | bytes 393248 | tf_op jit(solution)/shard_map/ppermute | solution.py:418
  194.5 7.7 %collective-permute-done.12 = bf16[96,2048]{1,0:T(8,128)(2,1)S(1)} collective-permute-done((bf16[96,2048]{1,0:T(8,128)(2,1)S(1)}, bf16[96,2048]{1,0:T(8,128)(2,1)S(1)}, u32[]{:S(2)}, u32[]{:S(2)}) %collective-permute-start.12) | collective-permute-done | bytes 393248 | tf_op jit(solution)/shard_map/ppermute | solution.py:418
  202.5 2.5 %collective-permute-start.22 = (bf16[48,2048]{1,0:T(8,128)(2,1)S(1)}, bf16[48,2048]{1,0:T(8,128)(2,1)S(1)}, u32[]{:S(2)}, u32[]{:S(2)}) collective-permute-start(bf16[48,2048]{1,0:T(8,128)(2,1)S(1)} %get-tuple-element.61), channel_id=1, source_target_pairs={{12,0},{8,4},{4,8},{0,12},{28,16},{24,20},{20,24},{16,28},{13,1},{... | collective-permute-start | bytes 589832 | tf_op jit(solution)/shard_map/ppermute | solution.py:433
  206.2 4.1 %collective-permute-done.30.refs_4_ = bf16[48,2048]{1,0:T(8,128)(2,1)S(1)} collective-permute-done((bf16[48,2048]{1,0:T(8,128)(2,1)S(1)}, bf16[48,2048]{1,0:T(8,128)(2,1)S(1)}, u32[]{:S(2)}, u32[]{:S(2)}) %collective-permute-start.30) | collective-permute-done | bytes 196640 | tf_op jit(solution)/shard_map/ppermute | solution.py:433
  210.2 1.8 collective-permute-done.31.refs_5_
  212.0 4.7 %collective-permute-done.21.refs_2_ = bf16[48,2048]{1,0:T(8,128)(2,1)S(1)} collective-permute-done((bf16[48,2048]{1,0:T(8,128)(2,1)S(1)}, bf16[48,2048]{1,0:T(8,128)(2,1)S(1)}, u32[]{:S(2)}, u32[]{:S(2)}) %collective-permute-start.21) | collective-permute-done | bytes 196640 | tf_op jit(solution)/shard_map/ppermute | solution.py:433
  216.7 3.4 %collective-permute-done.22.refs_3_ = bf16[48,2048]{1,0:T(8,128)(2,1)S(1)} collective-permute-done((bf16[48,2048]{1,0:T(8,128)(2,1)S(1)}, bf16[48,2048]{1,0:T(8,128)(2,1)S(1)}, u32[]{:S(2)}, u32[]{:S(2)}) %collective-permute-start.22) | collective-permute-done | bytes 196640 | tf_op jit(solution)/shard_map/ppermute | solution.py:433
  220.1 2.1 combine.1
  (103 shorter events, 15.7 us)
Async XLA Ops:
  0.0 56.5 %copy-start.8 = (f32[2]{0:T(128)S(1)}, f32[2]{0:T(128)}, u32[]{:S(2)}) copy-start(f32[2]{0:T(128)} %lam_ref.3) | copy-start | bytes 28
  3.5 47.8 %all-to-all-start = ((bf16[8,128,384]{2,1,0:T(8,128)(2,1)}), bf16[8,128,384]{2,1,0:T(8,128)(2,1)S(1)}, u32[]{:S(2)}, u32[]{:S(2)}) async-start(bf16[8,128,384]{2,1,0:T(8,128)(2,1)} %get-tuple-element.31), calls=%async_computation | async-start | bytes 1572864 | tf_op jit(solution)/shard_map/all_to_all | solution.py:284
  10.8 9.8 %collective-permute-start = (bf16[128,384]{1,0:T(8,128)(2,1)S(1)}, bf16[128,384]{1,0:T(8,128)(2,1)S(1)}, u32[]{:S(2)}, u32[]{:S(2)}) collective-permute-start(bf16[128,384]{1,0:T(8,128)(2,1)S(1)} %get-tuple-element.33), channel_id=1, source_target_pairs={{0,4},{4,0},{8,12},{12,8},{16,20},{20,16},{24,28},{28,24},{1,5},{5... | collective-permute-start | bytes 294920 | tf_op jit(solution)/shard_map/ppermute | solution.py:289
  12.8 14.0 %collective-permute-start.1 = (bf16[128,384]{1,0:T(8,128)(2,1)S(1)}, bf16[128,384]{1,0:T(8,128)(2,1)S(1)}, u32[]{:S(2)}, u32[]{:S(2)}) collective-permute-start(bf16[128,384]{1,0:T(8,128)(2,1)S(1)} %get-tuple-element.34), channel_id=1, source_target_pairs={{0,8},{4,12},{8,0},{12,4},{16,24},{20,28},{24,16},{28,20},{1,9},{5... | collective-permute-start | bytes 294920 | tf_op jit(solution)/shard_map/ppermute | solution.py:289
  14.3 17.3 %collective-permute-start.2 = (bf16[128,384]{1,0:T(8,128)(2,1)S(1)}, bf16[128,384]{1,0:T(8,128)(2,1)S(1)}, u32[]{:S(2)}, u32[]{:S(2)}) collective-permute-start(bf16[128,384]{1,0:T(8,128)(2,1)S(1)} %get-tuple-element.35), channel_id=1, source_target_pairs={{0,12},{4,8},{8,4},{12,0},{16,28},{20,24},{24,20},{28,16},{1,13},{... | collective-permute-start | bytes 294920 | tf_op jit(solution)/shard_map/ppermute | solution.py:289
  14.3 28.5 %collective-permute-start.3 = (bf16[128,384]{1,0:T(8,128)(2,1)S(1)}, bf16[128,384]{1,0:T(8,128)(2,1)S(1)}, u32[]{:S(2)}, u32[]{:S(2)}) collective-permute-start(bf16[128,384]{1,0:T(8,128)(2,1)S(1)} %get-tuple-element.36), channel_id=1, source_target_pairs={{0,16},{4,20},{8,24},{12,28},{16,0},{20,4},{24,8},{28,12},{1,17},{... | collective-permute-start | bytes 294920 | tf_op jit(solution)/shard_map/ppermute | solution.py:289
  17.2 28.2 %collective-permute-start.4 = (bf16[128,384]{1,0:T(8,128)(2,1)S(1)}, bf16[128,384]{1,0:T(8,128)(2,1)S(1)}, u32[]{:S(2)}, u32[]{:S(2)}) collective-permute-start(bf16[128,384]{1,0:T(8,128)(2,1)S(1)} %get-tuple-element.37), channel_id=1, source_target_pairs={{0,20},{4,16},{8,28},{12,24},{16,4},{20,0},{24,12},{28,8},{1,21},{... | collective-permute-start | bytes 294920 | tf_op jit(solution)/shard_map/ppermute | solution.py:289
  20.6 24.8 %collective-permute-start.5 = (bf16[128,384]{1,0:T(8,128)(2,1)S(1)}, bf16[128,384]{1,0:T(8,128)(2,1)S(1)}, u32[]{:S(2)}, u32[]{:S(2)}) collective-permute-start(bf16[128,384]{1,0:T(8,128)(2,1)S(1)} %get-tuple-element.38), channel_id=1, source_target_pairs={{0,24},{4,28},{8,16},{12,20},{16,8},{20,12},{24,0},{28,4},{1,25},{... | collective-permute-start | bytes 294920 | tf_op jit(solution)/shard_map/ppermute | solution.py:289
  26.8 18.6 %collective-permute-start.6 = (bf16[128,384]{1,0:T(8,128)(2,1)S(1)}, bf16[128,384]{1,0:T(8,128)(2,1)S(1)}, u32[]{:S(2)}, u32[]{:S(2)}) collective-permute-start(bf16[128,384]{1,0:T(8,128)(2,1)S(1)} %get-tuple-element.39), channel_id=1, source_target_pairs={{0,28},{4,24},{8,20},{12,16},{16,12},{20,8},{24,4},{28,0},{1,29},{... | collective-permute-start | bytes 294920 | tf_op jit(solution)/shard_map/ppermute | solution.py:289
  51.4 14.1 %all-to-all-start.2 = ((bf16[8,128,128]{2,1,0:T(8,128)(2,1)}), bf16[8,128,128]{2,1,0:T(8,128)(2,1)S(1)}, u32[]{:S(2)}, u32[]{:S(2)}) async-start(bf16[8,128,128]{2,1,0:T(8,128)(2,1)} %shard_map.146), calls=%async_computation.2 | async-start | bytes 524288 | tf_op jit(solution)/shard_map/all_to_all | solution.py:312
  65.5 12.2 %all-to-all-start.1 = ((bf16[8,128,128]{2,1,0:T(8,128)(2,1)}), bf16[8,128,128]{2,1,0:T(8,128)(2,1)S(1)}, u32[]{:S(2)}, u32[]{:S(2)}) async-start(bf16[8,128,128]{2,1,0:T(8,128)(2,1)} %shard_map.145), calls=%async_computation.1 | async-start | bytes 524288 | tf_op jit(solution)/shard_map/all_to_all | solution.py:312
  77.7 57.2 %copy-start.1 = (bf16[1,2048,1024]{2,1,0:T(8,128)(2,1)S(1)}, bf16[1,2048,1024]{2,1,0:T(8,128)(2,1)}, u32[]{:S(2)}) copy-start(bf16[1,2048,1024]{2,1,0:T(8,128)(2,1)} %refs_4_.7) | copy-start | bytes 12582916
  77.7 57.2 %copy-start.2 = (bf16[1,2048,1024]{2,1,0:T(8,128)(2,1)S(1)}, bf16[1,2048,1024]{2,1,0:T(8,128)(2,1)}, u32[]{:S(2)}) copy-start(bf16[1,2048,1024]{2,1,0:T(8,128)(2,1)} %refs_5_.7) | copy-start | bytes 12582916
  77.7 57.2 %copy-start.3 = (bf16[1,1024,2048]{2,1,0:T(8,128)(2,1)S(1)}, bf16[1,1024,2048]{2,1,0:T(8,128)(2,1)}, u32[]{:S(2)}) copy-start(bf16[1,1024,2048]{2,1,0:T(8,128)(2,1)} %refs_6_.7) | copy-start | bytes 12582916
  83.6 9.4 %collective-permute-start.32 = (bf16[48,2048]{1,0:T(8,128)(2,1)S(1)}, bf16[48,2048]{1,0:T(8,128)(2,1)S(1)}, u32[]{:S(2)}, u32[]{:S(2)}) collective-permute-start(bf16[48,2048]{1,0:T(8,128)(2,1)S(1)} %get-tuple-element.52), channel_id=1, source_target_pairs={{0,24},{4,28},{8,16},{12,20},{16,8},{20,12},{24,0},{28,4},{1,25},{... | collective-permute-start | bytes 589832 | tf_op jit(solution)/shard_map/ppermute | solution.py:426
  84.8 23.2 %collective-permute-start.33 = (bf16[48,2048]{1,0:T(8,128)(2,1)S(1)}, bf16[48,2048]{1,0:T(8,128)(2,1)S(1)}, u32[]{:S(2)}, u32[]{:S(2)}) collective-permute-start(bf16[48,2048]{1,0:T(8,128)(2,1)S(1)} %get-tuple-element.53), channel_id=1, source_target_pairs={{0,28},{4,24},{8,20},{12,16},{16,12},{20,8},{24,4},{28,0},{1,29},{... | collective-permute-start | bytes 589832 | tf_op jit(solution)/shard_map/ppermute | solution.py:426
  88.4 27.2 %collective-permute-start.23 = (bf16[48,2048]{1,0:T(8,128)(2,1)S(1)}, bf16[48,2048]{1,0:T(8,128)(2,1)S(1)}, u32[]{:S(2)}, u32[]{:S(2)}) collective-permute-start(bf16[48,2048]{1,0:T(8,128)(2,1)S(1)} %get-tuple-element.48), channel_id=1, source_target_pairs={{0,16},{4,20},{8,24},{12,28},{16,0},{20,4},{24,8},{28,12},{1,17},{... | collective-permute-start | bytes 589832 | tf_op jit(solution)/shard_map/ppermute | solution.py:426
  88.4 30.1 %collective-permute-start.24 = (bf16[48,2048]{1,0:T(8,128)(2,1)S(1)}, bf16[48,2048]{1,0:T(8,128)(2,1)S(1)}, u32[]{:S(2)}, u32[]{:S(2)}) collective-permute-start(bf16[48,2048]{1,0:T(8,128)(2,1)S(1)} %get-tuple-element.49), channel_id=1, source_target_pairs={{0,20},{4,16},{8,28},{12,24},{16,4},{20,0},{24,12},{28,8},{1,21},{... | collective-permute-start | bytes 589832 | tf_op jit(solution)/shard_map/ppermute | solution.py:426
  91.3 27.2 %collective-permute-start.14 = (bf16[48,2048]{1,0:T(8,128)(2,1)S(1)}, bf16[48,2048]{1,0:T(8,128)(2,1)S(1)}, u32[]{:S(2)}, u32[]{:S(2)}) collective-permute-start(bf16[48,2048]{1,0:T(8,128)(2,1)S(1)} %get-tuple-element.44), channel_id=1, source_target_pairs={{0,8},{4,12},{8,0},{12,4},{16,24},{20,28},{24,16},{28,20},{1,9},{5... | collective-permute-start | bytes 589832 | tf_op jit(solution)/shard_map/ppermute | solution.py:426
  93.0 27.2 %collective-permute-start.15 = (bf16[48,2048]{1,0:T(8,128)(2,1)S(1)}, bf16[48,2048]{1,0:T(8,128)(2,1)S(1)}, u32[]{:S(2)}, u32[]{:S(2)}) collective-permute-start(bf16[48,2048]{1,0:T(8,128)(2,1)S(1)} %get-tuple-element.45), channel_id=1, source_target_pairs={{0,12},{4,8},{8,4},{12,0},{16,28},{20,24},{24,20},{28,16},{1,13},{... | collective-permute-start | bytes 589832 | tf_op jit(solution)/shard_map/ppermute | solution.py:426
  108.0 17.0 %collective-permute-start.7 = (bf16[48,2048]{1,0:T(8,128)(2,1)S(1)}, bf16[48,2048]{1,0:T(8,128)(2,1)S(1)}, u32[]{:S(2)}, u32[]{:S(2)}) collective-permute-start(bf16[48,2048]{1,0:T(8,128)(2,1)S(1)} %get-tuple-element.41), channel_id=1, source_target_pairs={{0,4},{4,0},{8,12},{12,8},{16,20},{20,16},{24,28},{28,24},{1,5},{5... | collective-permute-start | bytes 589832 | tf_op jit(solution)/shard_map/ppermute | solution.py:426
  115.6 9.4 %collective-permute-start.34 = (bf16[96,2048]{1,0:T(8,128)(2,1)S(1)}, bf16[96,2048]{1,0:T(8,128)(2,1)S(1)}, u32[]{:S(2)}, u32[]{:S(2)}) collective-permute-start(bf16[96,2048]{1,0:T(8,128)(2,1)S(1)} %constant_dynamic-update-slice_fusion.6.refs_0_), channel_id=1, source_target_pairs={{0,2},{1,3},{2,0},{3,1},{4,6},{5,7},{6,4},{7,5},{8,10},{9,11},{10,... | collective-permute-start | bytes 1179656 | tf_op jit(solution)/shard_map/ppermute | solution.py:392
  118.5 8.1 %collective-permute-start.35 = (bf16[96,2048]{1,0:T(8,128)(2,1)S(1)}, bf16[96,2048]{1,0:T(8,128)(2,1)S(1)}, u32[]{:S(2)}, u32[]{:S(2)}) collective-permute-start(bf16[96,2048]{1,0:T(8,128)(2,1)S(1)} %constant_dynamic-update-slice_fusion.6.refs_0_), channel_id=1, source_target_pairs={{0,1},{1,0},{2,3},{3,2},{4,5},{5,4},{6,7},{7,6},{8,9},{9,8},{10,11... | collective-permute-start | bytes 1179656 | tf_op jit(solution)/shard_map/ppermute | solution.py:395
  118.5 14.8 %collective-permute-start.25 = (bf16[96,2048]{1,0:T(8,128)(2,1)S(1)}, bf16[96,2048]{1,0:T(8,128)(2,1)S(1)}, u32[]{:S(2)}, u32[]{:S(2)}) collective-permute-start(bf16[96,2048]{1,0:T(8,128)(2,1)S(1)} %constant_dynamic-update-slice_fusion.4.refs_0_), channel_id=1, source_target_pairs={{0,2},{1,3},{2,0},{3,1},{4,6},{5,7},{6,4},{7,5},{8,10},{9,11},{10,... | collective-permute-start | bytes 1179656 | tf_op jit(solution)/shard_map/ppermute | solution.py:392
  120.2 19.9 %collective-permute-start.26 = (bf16[96,2048]{1,0:T(8,128)(2,1)S(1)}, bf16[96,2048]{1,0:T(8,128)(2,1)S(1)}, u32[]{:S(2)}, u32[]{:S(2)}) collective-permute-start(bf16[96,2048]{1,0:T(8,128)(2,1)S(1)} %constant_dynamic-update-slice_fusion.4.refs_0_), channel_id=1, source_target_pairs={{0,1},{1,0},{2,3},{3,2},{4,5},{5,4},{6,7},{7,6},{8,9},{9,8},{10,11... | collective-permute-start | bytes 1179656 | tf_op jit(solution)/shard_map/ppermute | solution.py:395
  125.0 10.0 %collective-permute-start.36 = (bf16[96,2048]{1,0:T(8,128)(2,1)S(1)}, bf16[96,2048]{1,0:T(8,128)(2,1)S(1)}, u32[]{:S(2)}, u32[]{:S(2)}) collective-permute-start(bf16[96,2048]{1,0:T(8,128)(2,1)S(1)} %collective-permute-done.34.refs_1_), channel_id=1, source_target_pairs={{0,1},{1,0},{2,3},{3,2},{4,5},{5,4},{6,7},{7,6},{8,9},{9,8},{10,11... | collective-permute-start | bytes 1179656 | tf_op jit(solution)/shard_map/ppermute | solution.py:395
  125.0 16.8 %collective-permute-start.16 = (bf16[96,2048]{1,0:T(8,128)(2,1)S(1)}, bf16[96,2048]{1,0:T(8,128)(2,1)S(1)}, u32[]{:S(2)}, u32[]{:S(2)}) collective-permute-start(bf16[96,2048]{1,0:T(8,128)(2,1)S(1)} %constant_dynamic-update-slice_fusion.2.refs_0_), channel_id=1, source_target_pairs={{0,2},{1,3},{2,0},{3,1},{4,6},{5,7},{6,4},{7,5},{8,10},{9,11},{10,... | collective-permute-start | bytes 1179656 | tf_op jit(solution)/shard_map/ppermute | solution.py:392
  126.6 27.6 %collective-permute-start.17 = (bf16[96,2048]{1,0:T(8,128)(2,1)S(1)}, bf16[96,2048]{1,0:T(8,128)(2,1)S(1)}, u32[]{:S(2)}, u32[]{:S(2)}) collective-permute-start(bf16[96,2048]{1,0:T(8,128)(2,1)S(1)} %constant_dynamic-update-slice_fusion.2.refs_0_), channel_id=1, source_target_pairs={{0,1},{1,0},{2,3},{3,2},{4,5},{5,4},{6,7},{7,6},{8,9},{9,8},{10,11... | collective-permute-start | bytes 1179656 | tf_op jit(solution)/shard_map/ppermute | solution.py:395
  133.4 15.2 %collective-permute-start.8 = (bf16[96,2048]{1,0:T(8,128)(2,1)S(1)}, bf16[96,2048]{1,0:T(8,128)(2,1)S(1)}, u32[]{:S(2)}, u32[]{:S(2)}) collective-permute-start(bf16[96,2048]{1,0:T(8,128)(2,1)S(1)} %constant_dynamic-update-slice_fusion.refs_0_), channel_id=1, source_target_pairs={{0,2},{1,3},{2,0},{3,1},{4,6},{5,7},{6,4},{7,5},{8,10},{9,11},{10,... | collective-permute-start | bytes 1179656 | tf_op jit(solution)/shard_map/ppermute | solution.py:392
  134.9 13.7 %collective-permute-start.27 = (bf16[96,2048]{1,0:T(8,128)(2,1)S(1)}, bf16[96,2048]{1,0:T(8,128)(2,1)S(1)}, u32[]{:S(2)}, u32[]{:S(2)}) collective-permute-start(bf16[96,2048]{1,0:T(8,128)(2,1)S(1)} %collective-permute-done.25.refs_1_), channel_id=1, source_target_pairs={{0,1},{1,0},{2,3},{3,2},{4,5},{5,4},{6,7},{7,6},{8,9},{9,8},{10,11... | collective-permute-start | bytes 1179656 | tf_op jit(solution)/shard_map/ppermute | solution.py:395
  140.0 20.1 %collective-permute-start.9 = (bf16[96,2048]{1,0:T(8,128)(2,1)S(1)}, bf16[96,2048]{1,0:T(8,128)(2,1)S(1)}, u32[]{:S(2)}, u32[]{:S(2)}) collective-permute-start(bf16[96,2048]{1,0:T(8,128)(2,1)S(1)} %constant_dynamic-update-slice_fusion.refs_0_), channel_id=1, source_target_pairs={{0,1},{1,0},{2,3},{3,2},{4,5},{5,4},{6,7},{7,6},{8,9},{9,8},{10,11... | collective-permute-start | bytes 1179656 | tf_op jit(solution)/shard_map/ppermute | solution.py:395
  141.8 12.5 %collective-permute-start.18 = (bf16[96,2048]{1,0:T(8,128)(2,1)S(1)}, bf16[96,2048]{1,0:T(8,128)(2,1)S(1)}, u32[]{:S(2)}, u32[]{:S(2)}) collective-permute-start(bf16[96,2048]{1,0:T(8,128)(2,1)S(1)} %collective-permute-done.16.refs_1_), channel_id=1, source_target_pairs={{0,1},{1,0},{2,3},{3,2},{4,5},{5,4},{6,7},{7,6},{8,9},{9,8},{10,11... | collective-permute-start | bytes 1179656 | tf_op jit(solution)/shard_map/ppermute | solution.py:395
  148.6 11.6 %collective-permute-start.10 = (bf16[96,2048]{1,0:T(8,128)(2,1)S(1)}, bf16[96,2048]{1,0:T(8,128)(2,1)S(1)}, u32[]{:S(2)}, u32[]{:S(2)}) collective-permute-start(bf16[96,2048]{1,0:T(8,128)(2,1)S(1)} %collective-permute-done.8.refs_1_), channel_id=1, source_target_pairs={{0,1},{1,0},{2,3},{3,2},{4,5},{5,4},{6,7},{7,6},{8,9},{9,8},{10,11... | collective-permute-start | bytes 1179656 | tf_op jit(solution)/shard_map/ppermute | solution.py:395
  148.6 16.7 %collective-permute-start.37 = (bf16[2,96,2048]{2,1,0:T(8,128)(2,1)S(1)}, bf16[2,96,2048]{2,1,0:T(8,128)(2,1)S(1)}, u32[]{:S(2)}, u32[]{:S(2)}) collective-permute-start(bf16[2,96,2048]{2,1,0:T(8,128)(2,1)S(1)} %get-tuple-element.55), channel_id=1, source_target_pairs={{0,1},{1,0},{2,3},{3,2},{4,5},{5,4},{6,7},{7,6},{8,9},{9,8},{10,11... | collective-permute-start | bytes 2359304 | tf_op jit(solution)/shard_map/ppermute | solution.py:414
  154.2 12.8 %collective-permute-start.28 = (bf16[2,96,2048]{2,1,0:T(8,128)(2,1)S(1)}, bf16[2,96,2048]{2,1,0:T(8,128)(2,1)S(1)}, u32[]{:S(2)}, u32[]{:S(2)}) collective-permute-start(bf16[2,96,2048]{2,1,0:T(8,128)(2,1)S(1)} %get-tuple-element.51), channel_id=1, source_target_pairs={{0,1},{1,0},{2,3},{3,2},{4,5},{5,4},{6,7},{7,6},{8,9},{9,8},{10,11... | collective-permute-start | bytes 2359304 | tf_op jit(solution)/shard_map/ppermute | solution.py:414
  159.6 8.1 %collective-permute-start.19 = (bf16[2,96,2048]{2,1,0:T(8,128)(2,1)S(1)}, bf16[2,96,2048]{2,1,0:T(8,128)(2,1)S(1)}, u32[]{:S(2)}, u32[]{:S(2)}) collective-permute-start(bf16[2,96,2048]{2,1,0:T(8,128)(2,1)S(1)} %get-tuple-element.47), channel_id=1, source_target_pairs={{0,1},{1,0},{2,3},{3,2},{4,5},{5,4},{6,7},{7,6},{8,9},{9,8},{10,11... | collective-permute-start | bytes 2359304 | tf_op jit(solution)/shard_map/ppermute | solution.py:414
  165.2 4.2 %collective-permute-start.11 = (bf16[2,96,2048]{2,1,0:T(8,128)(2,1)S(1)}, bf16[2,96,2048]{2,1,0:T(8,128)(2,1)S(1)}, u32[]{:S(2)}, u32[]{:S(2)}) collective-permute-start(bf16[2,96,2048]{2,1,0:T(8,128)(2,1)S(1)} %get-tuple-element.43), channel_id=1, source_target_pairs={{0,1},{1,0},{2,3},{3,2},{4,5},{5,4},{6,7},{7,6},{8,9},{9,8},{10,11... | collective-permute-start | bytes 2359304 | tf_op jit(solution)/shard_map/ppermute | solution.py:414
  165.5 12.1 %collective-permute-start.38 = (bf16[96,2048]{1,0:T(8,128)(2,1)S(1)}, bf16[96,2048]{1,0:T(8,128)(2,1)S(1)}, u32[]{:S(2)}, u32[]{:S(2)}) collective-permute-start(bf16[96,2048]{1,0:T(8,128)(2,1)S(1)} %fusion.7), channel_id=1, source_target_pairs={{0,2},{1,3},{2,0},{3,1},{4,6},{5,7},{6,4},{7,5},{8,10},{9,11},{10,... | collective-permute-start | bytes 1179656 | tf_op jit(solution)/shard_map/ppermute | solution.py:418
  167.1 18.8 %collective-permute-start.29 = (bf16[96,2048]{1,0:T(8,128)(2,1)S(1)}, bf16[96,2048]{1,0:T(8,128)(2,1)S(1)}, u32[]{:S(2)}, u32[]{:S(2)}) collective-permute-start(bf16[96,2048]{1,0:T(8,128)(2,1)S(1)} %fusion.6), channel_id=1, source_target_pairs={{0,2},{1,3},{2,0},{3,1},{4,6},{5,7},{6,4},{7,5},{8,10},{9,11},{10,... | collective-permute-start | bytes 1179656 | tf_op jit(solution)/shard_map/ppermute | solution.py:418
  167.8 26.5 %collective-permute-start.20 = (bf16[96,2048]{1,0:T(8,128)(2,1)S(1)}, bf16[96,2048]{1,0:T(8,128)(2,1)S(1)}, u32[]{:S(2)}, u32[]{:S(2)}) collective-permute-start(bf16[96,2048]{1,0:T(8,128)(2,1)S(1)} %fusion.5), channel_id=1, source_target_pairs={{0,2},{1,3},{2,0},{3,1},{4,6},{5,7},{6,4},{7,5},{8,10},{9,11},{10,... | collective-permute-start | bytes 1179656 | tf_op jit(solution)/shard_map/ppermute | solution.py:418
  169.5 32.8 %collective-permute-start.12 = (bf16[96,2048]{1,0:T(8,128)(2,1)S(1)}, bf16[96,2048]{1,0:T(8,128)(2,1)S(1)}, u32[]{:S(2)}, u32[]{:S(2)}) collective-permute-start(bf16[96,2048]{1,0:T(8,128)(2,1)S(1)} %fusion.4), channel_id=1, source_target_pairs={{0,2},{1,3},{2,0},{3,1},{4,6},{5,7},{6,4},{7,5},{8,10},{9,11},{10,... | collective-permute-start | bytes 1179656 | tf_op jit(solution)/shard_map/ppermute | solution.py:418
  177.7 24.8 %collective-permute-start.39 = (bf16[48,2048]{1,0:T(8,128)(2,1)S(1)}, bf16[48,2048]{1,0:T(8,128)(2,1)S(1)}, u32[]{:S(2)}, u32[]{:S(2)}) collective-permute-start(bf16[48,2048]{1,0:T(8,128)(2,1)S(1)} %get-tuple-element.58), channel_id=1, source_target_pairs={{24,0},{28,4},{16,8},{20,12},{8,16},{12,20},{0,24},{4,28},{25,1},{... | collective-permute-start | bytes 589832 | tf_op jit(solution)/shard_map/ppermute | solution.py:433
  180.5 24.5 %collective-permute-start.40 = (bf16[48,2048]{1,0:T(8,128)(2,1)S(1)}, bf16[48,2048]{1,0:T(8,128)(2,1)S(1)}, u32[]{:S(2)}, u32[]{:S(2)}) collective-permute-start(bf16[48,2048]{1,0:T(8,128)(2,1)S(1)} %get-tuple-element.57), channel_id=1, source_target_pairs={{28,0},{24,4},{20,8},{16,12},{12,16},{8,20},{4,24},{0,28},{29,1},{... | collective-permute-start | bytes 589832 | tf_op jit(solution)/shard_map/ppermute | solution.py:433
  186.1 24.1 %collective-permute-start.30 = (bf16[48,2048]{1,0:T(8,128)(2,1)S(1)}, bf16[48,2048]{1,0:T(8,128)(2,1)S(1)}, u32[]{:S(2)}, u32[]{:S(2)}) collective-permute-start(bf16[48,2048]{1,0:T(8,128)(2,1)S(1)} %get-tuple-element.60), channel_id=1, source_target_pairs={{16,0},{20,4},{24,8},{28,12},{0,16},{4,20},{8,24},{12,28},{17,1},{... | collective-permute-start | bytes 589832 | tf_op jit(solution)/shard_map/ppermute | solution.py:433
  194.4 17.7 %collective-permute-start.31 = (bf16[48,2048]{1,0:T(8,128)(2,1)S(1)}, bf16[48,2048]{1,0:T(8,128)(2,1)S(1)}, u32[]{:S(2)}, u32[]{:S(2)}) collective-permute-start(bf16[48,2048]{1,0:T(8,128)(2,1)S(1)} %get-tuple-element.59), channel_id=1, source_target_pairs={{20,0},{16,4},{28,8},{24,12},{4,16},{0,20},{12,24},{8,28},{21,1},{... | collective-permute-start | bytes 589832 | tf_op jit(solution)/shard_map/ppermute | solution.py:433
  202.3 14.4 %collective-permute-start.21 = (bf16[48,2048]{1,0:T(8,128)(2,1)S(1)}, bf16[48,2048]{1,0:T(8,128)(2,1)S(1)}, u32[]{:S(2)}, u32[]{:S(2)}) collective-permute-start(bf16[48,2048]{1,0:T(8,128)(2,1)S(1)} %get-tuple-element.62), channel_id=1, source_target_pairs={{8,0},{12,4},{0,8},{4,12},{24,16},{28,20},{16,24},{20,28},{9,1},{1... | collective-permute-start | bytes 589832 | tf_op jit(solution)/shard_map/ppermute | solution.py:433
  202.5 17.6 %collective-permute-start.22 = (bf16[48,2048]{1,0:T(8,128)(2,1)S(1)}, bf16[48,2048]{1,0:T(8,128)(2,1)S(1)}, u32[]{:S(2)}, u32[]{:S(2)}) collective-permute-start(bf16[48,2048]{1,0:T(8,128)(2,1)S(1)} %get-tuple-element.61), channel_id=1, source_target_pairs={{12,0},{8,4},{4,8},{0,12},{28,16},{24,20},{20,24},{16,28},{13,1},{... | collective-permute-start | bytes 589832 | tf_op jit(solution)/shard_map/ppermute | solution.py:433
  205.0 15.1 %collective-permute-start.13 = (bf16[48,2048]{1,0:T(8,128)(2,1)S(1)}, bf16[48,2048]{1,0:T(8,128)(2,1)S(1)}, u32[]{:S(2)}, u32[]{:S(2)}) collective-permute-start(bf16[48,2048]{1,0:T(8,128)(2,1)S(1)} %get-tuple-element.63), channel_id=1, source_target_pairs={{4,0},{0,4},{12,8},{8,12},{20,16},{16,20},{28,24},{24,28},{5,1},{1... | collective-permute-start | bytes 589832 | tf_op jit(solution)/shard_map/ppermute | solution.py:433
  (9 other events, 176.1 us)
where the time goes:
time: 223 us; the launch traced here: 222 us
  waiting for transfers between devices  95.9 us (43%)
  starting transfers between devices  78.2 us (35%)
  Pallas kernels  44.6 us (20%)
    ppermute x4, waiting for transfers between devices, gather_sums(): got = lax.ppermute(pair, 'dp', shift(rows_y - k))  27.2 us
    ppermute x7, starting transfers between devices, local(): arrived[k] = lax.ppermute(sent[k], 'sp', away(k)) if k else sent[k]  23.9 us
    pallas_call x4, Pallas kernels, expert(): pl.pallas_call(functools.partial(expert_kernel, pieces=pieces), in_specs=...  20.5 us
    ppermute x4, waiting for transfers between devices, spread(): here.append(lax.ppermute(rows, 'dp', shift(k)))  19 us
    ppermute x7, starting transfers between devices, local(): blocks[k] = lax.ppermute(blocks[k], 'sp', away(k))  17.5 us
    ppermute x7, waiting for transfers between devices, local(): blocks[k] = lax.ppermute(blocks[k], 'sp', away(k))  17.2 us
    ppermute x7, waiting for transfers between devices, local(): returned[k] = lax.ppermute(block, 'sp', back(k)) if k else block  14 us
    ppermute x7, waiting for transfers between devices, local(): arrived[k] = lax.ppermute(sent[k], 'sp', away(k)) if k else sent[k]  9.45 us
  transfers between devices with their start and end apart: 44, of which 21 were waited for; matrix products, arithmetic and copies ran while one was open for 1% of the time, Pallas kernels for 15%

commit v1 on v0

--- a/solution.py
+++ b/solution.py
@@ -9,7 +9,7 @@
 from jax.sharding import PartitionSpec as P
 
 
-PRICE = 32
+PRICE = 64
 
 F32 = jnp.float32
 BF16 = jnp.bfloat16
@@ -54,11 +54,12 @@
                     first_ref[k, :, lanes] = part
 
 
-def attention_kernel(own_ref, lam_ref, gain_ref, *refs, head, paired):
-    in_refs, o_ref = refs[:-1], refs[-1]
-    relative = len(in_refs) > 1
-    count = o_ref.shape[0]
-    width = o_ref.shape[2]
+def attention_kernel(lam_ref, gain_ref, *refs, head):
+    relative = len(refs) > 2
+    half = len(refs) // 2
+    in_refs, o_refs = refs[:half], refs[half:]
+    count = len(o_refs) if relative else o_refs[0].shape[0]
+    width = o_refs[0].shape[-1]
 
     def part(k, n):
         at = slice(n * width, (n + 1) * width)
@@ -69,7 +70,6 @@
     extended = jnp.concatenate([values, jnp.ones_like(values)], axis=1)
     gain = gain_ref[...]
     weight = lam_ref[head]
-    own = own_ref[0]
     for pair in range(count // 2):
         q = jnp.concatenate([part(2 * pair, 0), part(2 * pair + 1, 0)], axis=0)
         rows = q.shape[0]
@@ -91,8 +91,9 @@
         for n in range(2):
             k = 2 * pair + n
             if relative:
-                k = own ^ k if paired else (own - k + count) % count
-            o_ref[k] = out[n * (rows // 2) : (n + 1) * (rows // 2), :]
+                o_refs[k][...] = out[n * (rows // 2) : (n + 1) * (rows // 2), :]
+            else:
+                o_refs[0][k] = out[n * (rows // 2) : (n + 1) * (rows // 2), :]
 
 
 def rms(x, epsilon):
@@ -114,6 +115,23 @@
     @pl.when(step != 0)
     def _():
         out_ref[...] += update
+
+
+def near_kernel(own_ref, *refs, per_step):
+    del own_ref
+    head_refs, w_refs, out_ref = refs[: -per_step - 1], refs[-per_step - 1 : -1], refs[-1]
+    step = pl.program_id(0)
+    rhs = jnp.concatenate([w[0, 0] for w in w_refs], axis=0)
+    for i in range(len(head_refs) // per_step):
+
+        @pl.when(step == i)
+        def _(i=i):
+            lhs = jnp.concatenate([r[...] for r in head_refs[i * per_step : (i + 1) * per_step]], axis=1)
+            update = jnp.dot(lhs, rhs, preferred_element_type=F32)
+            if i:
+                out_ref[...] += update
+            else:
+                out_ref[...] = update
 
 
 def project_kernel(*refs, carried, experts):
@@ -210,6 +228,7 @@
 
 def group_list(sp_count):
     pairs = [(k, k + 1) for k in range(0, sp_count, 2)]
+    pairs = [pairs[0]] + [p[::-1] for p in pairs[1:]]
     return pairs[:1] + pairs[len(pairs) // 2 :][::-1] + pairs[1 : len(pairs) // 2]
 
 
@@ -297,31 +316,47 @@
     head_spec = pl.BlockSpec((sp_count, tokens, width), lambda i: (0, 0, 0))
     carry = []
     for j in [*range(1, heads), 0]:
+        near_head = j > 0
+        block = jax.ShapeDtypeStruct((tokens, width), BF16)
         head_out = pl.pallas_call(
-            functools.partial(attention_kernel, head=j, paired=paired),
-            in_specs=[smem, smem] + [vmem] * (1 + len(arrived[j])),
-            out_specs=vmem,
-            out_shape=jax.ShapeDtypeStruct((sp_count, tokens, width), BF16),
+            functools.partial(attention_kernel, head=j),
+            in_specs=[smem] + [vmem] * (1 + len(arrived[j])),
+            out_specs=[vmem] * sp_count if near_head else vmem,
+            out_shape=[block] * sp_count
+            if near_head
+            else jax.ShapeDtypeStruct((sp_count, tokens, width), BF16),
             compiler_params=params(16),
             cost_estimate=pl.CostEstimate(
-                flops=8 * length * length * width,
+                flops=PRICE * length * length * width,
                 bytes_accessed=8 * length * width,
                 transcendentals=2 * length * length,
             ),
-        )(own_row, lambdas, gain_row, *[on_chip(x) for x in arrived[j]])
-        token_head = lax.all_to_all(
-            head_out, "sp", split_axis=0, concat_axis=0, tiled=True
-        )
-        weight_spec = pl.BlockSpec(
-            (count, None, width, model_dim), functools.partial(lambda i, j: (i, j, 0, 0), j=j)
-        )
-        if j:
-            carry = [
+        )(lambdas, gain_row, *[on_chip(x) for x in arrived[j]])
+        if near_head:
+            head_out = list(head_out)
+            for k in range(1, sp_count):
+                head_out[k] = lax.ppermute(head_out[k], "sp", back(k))
+            per_step = 2
+
+            def weight_place(i, o, n=0, j=j):
+                k = i * per_step + n
+                return (o[0] ^ k if paired else (o[0] + k) % sp_count), j, 0, 0
+
+            carry.append(
                 pl.pallas_call(
-                    partial_kernel,
-                    grid=(steps,),
-                    in_specs=[head_spec, weight_spec] + [full] * len(carry),
-                    out_specs=full,
+                    functools.partial(near_kernel, per_step=per_step),
+                    grid_spec=pltpu.PrefetchScalarGridSpec(
+                        num_scalar_prefetch=1,
+                        grid=(sp_count // per_step,),
+                        in_specs=[vmem] * sp_count
+                        + [
+                            pl.BlockSpec(
+                                (1, 1, width, model_dim), functools.partial(weight_place, n=n)
+                            )
+                            for n in range(per_step)
+                        ],
+                        out_specs=pl.BlockSpec((tokens, model_dim), lambda i, o: (0, 0)),
+                    ),
                     out_shape=jax.ShapeDtypeStruct((tokens, model_dim), F32),
                     compiler_params=params(12),
                     cost_estimate=pl.CostEstimate(
@@ -329,8 +364,17 @@
                         bytes_accessed=2 * sp_count * width * model_dim,
                         transcendentals=0,
                     ),
-                )(token_head, weight_view, *carry)
-            ]
+                )(own_row, *[on_chip(x) for x in head_out], weight_view, weight_view)
+            )
+            continue
+        token_head = lax.all_to_all(
+            head_out, "sp", split_axis=0, concat_axis=0, tiled=True
+        )
+        weight_spec = pl.BlockSpec(
+            (count, None, width, model_dim), functools.partial(lambda i, j: (i, j, 0, 0), j=j)
+        )
+    if len(carry) > 1:
+        carry = [functools.reduce(jnp.add, carry)]
 
     experts = sp_count
     capacity = max(2, 3 * tokens // experts)

time: 223 us -> 215 us (0.964)
  waiting for transfers between devices: 95.9 us -> 85.5 us
  starting transfers between devices: 78.2 us -> 82.1 us
    ppermute x7, waiting for transfers between devices: 17.2 us -> 3.29 us  [local(): blocks[k] = lax.ppermute(blocks[k], 'sp', away(k))]
    ppermute x0 -> x7, starting transfers between devices: none -> 11.3 us  [local(): head_out[k] = lax.ppermute(head_out[k], 'sp', back(k))]
    all_to_all x1, waiting for transfers between devices: 0.01 us -> 9.18 us  [local(): lax.all_to_all(outgoing[0], 'sp', split_axis=0, concat_axis=0, tiled=True)]
    all_to_all x2 -> x1, waiting for transfers between devices: 9.06 us -> 0.01 us  [local(): lax.all_to_all(head_out, 'sp', split_axis=0, concat_axis=0, tiled=True)]
    all_to_all x2 -> x1, starting transfers between devices: 8.7 us -> 3.41 us  [local(): lax.all_to_all(head_out, 'sp', split_axis=0, concat_axis=0, tiled=True)]
    ppermute x0 -> x7, waiting for transfers between devices: none -> 3.32 us  [local(): head_out[k] = lax.ppermute(head_out[k], 'sp', back(k))]
    ppermute x7, starting transfers between devices: 23.9 us -> 21.4 us  [local(): arrived[k] = lax.ppermute(sent[k], 'sp', away(k)) if k else sent[k]]
  transfers between devices with their start and end apart: 44 -> 50, of which waited for: 21 -> 20; matrix products, arithmetic and copies ran while one was open for 1% -> 1% of each run, Pallas kernels for 15% -> 15%
where the time goes in v1:
time: 215 us
  waiting for transfers between devices  85.5 us (40%)
  starting transfers between devices  82.1 us (38%)
  Pallas kernels  43.6 us (20%)
    ppermute x4, waiting for transfers between devices, gather_sums(): got = lax.ppermute(pair, 'dp', shift(rows_y - k))  26.6 us
    ppermute x7, starting transfers between devices, local(): arrived[k] = lax.ppermute(sent[k], 'sp', away(k)) if k else sent[k]  21.4 us
    pallas_call x4, Pallas kernels, expert(): pl.pallas_call(functools.partial(expert_kernel, pieces=pieces), in_specs=...  20.5 us
    ppermute x4, waiting for transfers between devices, spread(): here.append(lax.ppermute(rows, 'dp', shift(k)))  20.1 us
    ppermute x7, starting transfers between devices, local(): blocks[k] = lax.ppermute(blocks[k], 'sp', away(k))  17.5 us
    ppermute x7, waiting for transfers between devices, local(): returned[k] = lax.ppermute(block, 'sp', back(k)) if k else block  13.2 us
    ppermute x7, starting transfers between devices, local(): head_out[k] = lax.ppermute(head_out[k], 'sp', back(k))  11.3 us
    ppermute x7, waiting for transfers between devices, local(): arrived[k] = lax.ppermute(sent[k], 'sp', away(k)) if k else sent[k]  9.71 us
  transfers between devices with their start and end apart: 50, of which 20 were waited for; matrix products, arithmetic and copies ran while one was open for 1% of the time, Pallas kernels for 15%

profile of v1, /device:TPU:0, one launch (start us, length us, event | category | flops | bytes accessed | tf_op | source)
XLA Modules:
  0.0 214.9 jit_solution(14708767112050933648)
XLA Ops:
  0.3 3.2 %lay.1 = (bf16[8,128,384]{2,1,0:T(8,128)(2,1)}, bf16[128,384]{1,0:T(8,128)(2,1)S(1)}, bf16[128,384]{1,0:T(8,128)(2,1)S(1)}, bf16[128,384]{1,0:T(8,128)(2,1)S(1)}...) custom-call(s32[1]{0:T(128)} %bitcast.1.own_ref, ...), custom_call_target="tpu_custom_call" | custom-call | tf_op jit(solution)/shard_map/lay/pallas_call | solution.py:283
  3.5 7.3 %all-to-all-start = ((bf16[8,128,384]{2,1,0:T(8,128)(2,1)}), bf16[8,128,384]{2,1,0:T(8,128)(2,1)S(1)}, u32[]{:S(2)}, u32[]{:S(2)}) async-start(bf16[8,128,384]{2,1,0:T(8,128)(2,1)} %get-tuple-element.39), calls=%async_computation | async-start | bytes 1572864 | tf_op jit(solution)/shard_map/all_to_all | solution.py:303
  10.8 2.0 collective-permute-start
  14.3 2.9 %collective-permute-start.3 = (bf16[128,384]{1,0:T(8,128)(2,1)S(1)}, bf16[128,384]{1,0:T(8,128)(2,1)S(1)}, u32[]{:S(2)}, u32[]{:S(2)}) collective-permute-start(bf16[128,384]{1,0:T(8,128)(2,1)S(1)} %get-tuple-element.44), channel_id=1, source_target_pairs={{0,16},{4,20},{8,24},{12,28},{16,0},{20,4},{24,8},{28,12},{1,17},{... | collective-permute-start | bytes 294920 | tf_op jit(solution)/shard_map/ppermute | solution.py:308
  18.7 1.9 collective-permute-done.refs_1_
  20.6 4.9 %collective-permute-start.5 = (bf16[128,384]{1,0:T(8,128)(2,1)S(1)}, bf16[128,384]{1,0:T(8,128)(2,1)S(1)}, u32[]{:S(2)}, u32[]{:S(2)}) collective-permute-start(bf16[128,384]{1,0:T(8,128)(2,1)S(1)} %get-tuple-element.46), channel_id=1, source_target_pairs={{0,24},{4,28},{8,16},{12,20},{16,8},{20,12},{24,0},{28,4},{1,25},{... | collective-permute-start | bytes 294920 | tf_op jit(solution)/shard_map/ppermute | solution.py:308
  26.9 4.7 %collective-permute-start.6 = (bf16[128,384]{1,0:T(8,128)(2,1)S(1)}, bf16[128,384]{1,0:T(8,128)(2,1)S(1)}, u32[]{:S(2)}, u32[]{:S(2)}) collective-permute-start(bf16[128,384]{1,0:T(8,128)(2,1)S(1)} %get-tuple-element.47), channel_id=1, source_target_pairs={{0,28},{4,24},{8,20},{12,16},{16,12},{20,8},{24,4},{28,0},{1,29},{... | collective-permute-start | bytes 294920 | tf_op jit(solution)/shard_map/ppermute | solution.py:308
  31.6 9.2 %all-to-all-done.refs_0_ = bf16[8,128,384]{2,1,0:T(8,128)(2,1)S(1)} async-done(((bf16[8,128,384]{2,1,0:T(8,128)(2,1)}), bf16[8,128,384]{2,1,0:T(8,128)(2,1)S(1)}, u32[]{:S(2)}, u32[]{:S(2)}) %all-to-all-start) | async-done | bytes 786464 | tf_op jit(solution)/shard_map/all_to_all | solution.py:303
  42.1 4.5 %shard_map.145 = bf16[8,128,128]{2,1,0:T(8,128)(2,1)} custom-call(f32[2]{0:T(128)S(1)} %copy-done.7, f32[1,128]{1,0:T(1,128)S(1)} %bitcast.43, bf16[8,128,384]{2,1,0:T(8,128)(2,1)S(1)} %all-to-all-done.refs_0_), custom_call_target="tpu_custom_call" | custom-call | flops 8589934592 | bytes 1048576 | tf_op jit(solution)/shard_map/pallas_call | solution.py:321
  46.6 3.4 %all-to-all-start.1 = ((bf16[8,128,128]{2,1,0:T(8,128)(2,1)}), bf16[8,128,128]{2,1,0:T(8,128)(2,1)S(1)}, u32[]{:S(2)}, u32[]{:S(2)}) async-start(bf16[8,128,128]{2,1,0:T(8,128)(2,1)} %shard_map.145), calls=%async_computation.1 | async-start | bytes 524288 | tf_op jit(solution)/shard_map/all_to_all | solution.py:370
  50.0 3.8 %shard_map.146 = (bf16[128,128]{1,0:T(8,128)(2,1)S(1)}, bf16[128,128]{1,0:T(8,128)(2,1)S(1)}, bf16[128,128]{1,0:T(8,128)(2,1)S(1)}, bf16[128,128]{1,0:T(8,128)(2...) custom-call(f32[2]{0:T(128)S(1)} %copy-done.8, ...), custom_call_target="tpu_custom_call" | custom-call | flops 8589934592 | bytes 1048576 | tf_op jit(solution)/shard_map/pallas_call | solution.py:321
  53.8 2.9 %collective-permute-start.10 = (bf16[128,128]{1,0:T(8,128)(2,1)S(1)}, bf16[128,128]{1,0:T(8,128)(2,1)S(1)}, u32[]{:S(2)}, u32[]{:S(2)}) collective-permute-start(bf16[128,128]{1,0:T(8,128)(2,1)S(1)} %get-tuple-element.52), channel_id=1, source_target_pairs={{16,0},{20,4},{24,8},{28,12},{0,16},{4,20},{8,24},{12,28},{17,1},{... | collective-permute-start | bytes 98312 | tf_op jit(solution)/shard_map/ppermute | solution.py:338
  58.3 3.4 %collective-permute-start.12 = (bf16[128,128]{1,0:T(8,128)(2,1)S(1)}, bf16[128,128]{1,0:T(8,128)(2,1)S(1)}, u32[]{:S(2)}, u32[]{:S(2)}) collective-permute-start(bf16[128,128]{1,0:T(8,128)(2,1)S(1)} %get-tuple-element.54), channel_id=1, source_target_pairs={{24,0},{28,4},{16,8},{20,12},{8,16},{12,20},{0,24},{4,28},{25,1},{... | collective-permute-start | bytes 98312 | tf_op jit(solution)/shard_map/ppermute | solution.py:338
  61.7 1.9 collective-permute-start.7
  63.6 1.6 collective-permute-start.9
  65.3 3.0 %collective-permute-done.13.refs_7_ = bf16[128,128]{1,0:T(8,128)(2,1)S(1)} collective-permute-done((bf16[128,128]{1,0:T(8,128)(2,1)S(1)}, bf16[128,128]{1,0:T(8,128)(2,1)S(1)}, u32[]{:S(2)}, u32[]{:S(2)}) %collective-permute-start.13) | collective-permute-done | bytes 32800 | tf_op jit(solution)/shard_map/ppermute | solution.py:338
  68.6 3.7 %shard_map.147.refs_6_ = f32[128,2048]{1,0:T(8,128)S(1)} custom-call(s32[1]{0:T(128)} %bitcast.1.own_ref, bf16[128,128]{1,0:T(8,128)(2,1)S(1)} %get-tuple-element.48.refs_0_, bf16[128,128]{1,0:T(8,128)(2,1)S(1)} %collective-permute-done.7.refs_1_, bf16[128,128]{1,0:T(8,128)(2,1)S(1)} %collective-permute-done.8.refs_2_, ...), custom_call_target="tpu_custom_call" | custom-call | flops 536870912 | bytes 4194304 | tf_op jit(solution)/shard_map/pallas_call | solution.py:346
  72.4 5.9 %project.1 = (bf16[128,2048]{1,0:T(8,128)(2,1)S(1)}, bf16[48,2048]{1,0:T(8,128)(2,1)S(1)}, bf16[48,2048]{1,0:T(8,128)(2,1)S(1)}, bf16[48,2048]{1,0:T(8,128)(2,1)...) custom-call(bf16[8,128,128]{2,1,0:T(8,128)(2,1)S(1)} %all-to-all-don, ...), custom_call_target="tpu_custom_call" | custom-call | flops 17179869184 | bytes 134217728 | tf_op jit(solution)/shard_map/project/pallas_call | solution.py:388
  78.3 3.6 %collective-permute-start.39 = (bf16[48,2048]{1,0:T(8,128)(2,1)S(1)}, bf16[48,2048]{1,0:T(8,128)(2,1)S(1)}, u32[]{:S(2)}, u32[]{:S(2)}) collective-permute-start(bf16[48,2048]{1,0:T(8,128)(2,1)S(1)} %get-tuple-element.68), channel_id=1, source_target_pairs={{0,28},{4,24},{8,20},{12,16},{16,12},{20,8},{24,4},{28,0},{1,29},{... | collective-permute-start | bytes 589832 | tf_op jit(solution)/shard_map/ppermute | solution.py:470
  82.5 2.5 %collective-permute-start.30 = (bf16[48,2048]{1,0:T(8,128)(2,1)S(1)}, bf16[48,2048]{1,0:T(8,128)(2,1)S(1)}, u32[]{:S(2)}, u32[]{:S(2)}) collective-permute-start(bf16[48,2048]{1,0:T(8,128)(2,1)S(1)} %get-tuple-element.64), channel_id=1, source_target_pairs={{0,20},{4,16},{8,28},{12,24},{16,4},{20,0},{24,12},{28,8},{1,21},{... | collective-permute-start | bytes 589832 | tf_op jit(solution)/shard_map/ppermute | solution.py:470
  87.2 1.7 collective-permute-done.39
  88.8 11.0 %collective-permute-start.22 = (bf16[48,2048]{1,0:T(8,128)(2,1)S(1)}, bf16[48,2048]{1,0:T(8,128)(2,1)S(1)}, u32[]{:S(2)}, u32[]{:S(2)}) collective-permute-start(bf16[48,2048]{1,0:T(8,128)(2,1)S(1)} %get-tuple-element.61), channel_id=1, source_target_pairs={{0,8},{4,12},{8,0},{12,4},{16,24},{20,28},{24,16},{28,20},{1,9},{5... | collective-permute-start | bytes 589832 | tf_op jit(solution)/shard_map/ppermute | solution.py:470
  99.9 1.5 collective-permute-start.14
  101.4 6.4 %collective-permute-done.30 = bf16[48,2048]{1,0:T(8,128)(2,1)S(1)} collective-permute-done((bf16[48,2048]{1,0:T(8,128)(2,1)S(1)}, bf16[48,2048]{1,0:T(8,128)(2,1)S(1)}, u32[]{:S(2)}, u32[]{:S(2)}) %collective-permute-start.30) | collective-permute-done | bytes 196640 | tf_op jit(solution)/shard_map/ppermute | solution.py:470
  107.9 1.5 collective-permute-start.41
  109.4 1.6 collective-permute-done.31
  111.0 1.6 collective-permute-start.32
  113.0 6.2 %collective-permute-done.41.refs_1_ = bf16[96,2048]{1,0:T(8,128)(2,1)S(1)} collective-permute-done((bf16[96,2048]{1,0:T(8,128)(2,1)S(1)}, bf16[96,2048]{1,0:T(8,128)(2,1)S(1)}, u32[]{:S(2)}, u32[]{:S(2)}) %collective-permute-start.41) | collective-permute-done | bytes 393248 | tf_op jit(solution)/shard_map/ppermute | solution.py:436
  119.2 1.5 collective-permute-start.23
  121.0 6.6 %collective-permute-done.32.refs_1_ = bf16[96,2048]{1,0:T(8,128)(2,1)S(1)} collective-permute-done((bf16[96,2048]{1,0:T(8,128)(2,1)S(1)}, bf16[96,2048]{1,0:T(8,128)(2,1)S(1)}, u32[]{:S(2)}, u32[]{:S(2)}) %collective-permute-start.32) | collective-permute-done | bytes 393248 | tf_op jit(solution)/shard_map/ppermute | solution.py:436
  129.0 5.1 %shard_map.151 = (bf16[2,96,2048]{2,1,0:T(8,128)(2,1)S(1)}, bf16[2,96,2048]{2,1,0:T(8,128)(2,1)S(1)}) custom-call(bf16[96,2048]{1,0:T(8,128)(2,1)S(1)} %constant_dynamic-update-slice_fusion.6.refs_0_, bf16[96,2048]{1,0:T(8,128)(2,1)S(1)} %collective-permute-done.41.refs_1_, bf16[96,2048]{1,0:T(8,128)(2,1)S(1)} %collective-permute-done.42.refs_2_, ...), custom_call_target="tpu_custom_call" | custom-call | flops 4831838208 | bytes 3145728 | tf_op jit(solution)/shard_map/pallas_call | solution.py:444
  136.0 6.0 %collective-permute-done.15.refs_1_ = bf16[96,2048]{1,0:T(8,128)(2,1)S(1)} collective-permute-done((bf16[96,2048]{1,0:T(8,128)(2,1)S(1)}, bf16[96,2048]{1,0:T(8,128)(2,1)S(1)}, u32[]{:S(2)}, u32[]{:S(2)}) %collective-permute-start.15) | collective-permute-done | bytes 393248 | tf_op jit(solution)/shard_map/ppermute | solution.py:436
  142.5 5.1 %shard_map.150 = (bf16[2,96,2048]{2,1,0:T(8,128)(2,1)S(1)}, bf16[2,96,2048]{2,1,0:T(8,128)(2,1)S(1)}) custom-call(bf16[96,2048]{1,0:T(8,128)(2,1)S(1)} %constant_dynamic-update-slice_fusion.4.refs_0_, bf16[96,2048]{1,0:T(8,128)(2,1)S(1)} %collective-permute-done.32.refs_1_, bf16[96,2048]{1,0:T(8,128)(2,1)S(1)} %collective-permute-done.33.refs_2_, ...), custom_call_target="tpu_custom_call" | custom-call | flops 4831838208 | bytes 3145728 | tf_op jit(solution)/shard_map/pallas_call | solution.py:444
  147.6 5.3 %shard_map.149 = (bf16[2,96,2048]{2,1,0:T(8,128)(2,1)S(1)}, bf16[2,96,2048]{2,1,0:T(8,128)(2,1)S(1)}) custom-call(bf16[96,2048]{1,0:T(8,128)(2,1)S(1)} %constant_dynamic-update-slice_fusion.2.refs_0_, bf16[96,2048]{1,0:T(8,128)(2,1)S(1)} %collective-permute-done.23.refs_1_, bf16[96,2048]{1,0:T(8,128)(2,1)S(1)} %collective-permute-done.24.refs_2_, ...), custom_call_target="tpu_custom_call" | custom-call | flops 4831838208 | bytes 3145728 | tf_op jit(solution)/shard_map/pallas_call | solution.py:444
  153.5 5.1 %shard_map.148 = (bf16[2,96,2048]{2,1,0:T(8,128)(2,1)S(1)}, bf16[2,96,2048]{2,1,0:T(8,128)(2,1)S(1)}) custom-call(bf16[96,2048]{1,0:T(8,128)(2,1)S(1)} %constant_dynamic-update-slice_fusion.refs_0_, bf16[96,2048]{1,0:T(8,128)(2,1)S(1)} %collective-permute-done.15.refs_1_, bf16[96,2048]{1,0:T(8,128)(2,1)S(1)} %collective-permute-done.16.refs_2_, ...), custom_call_target="tpu_custom_call" | custom-call | flops 4831838208 | bytes 3145728 | tf_op jit(solution)/shard_map/pallas_call | solution.py:444
  158.8 1.5 collective-permute-start.45
  161.2 1.5 collective-permute-start.27
  163.4 7.4 %collective-permute-done.45 = bf16[96,2048]{1,0:T(8,128)(2,1)S(1)} collective-permute-done((bf16[96,2048]{1,0:T(8,128)(2,1)S(1)}, bf16[96,2048]{1,0:T(8,128)(2,1)S(1)}, u32[]{:S(2)}, u32[]{:S(2)}) %collective-permute-start.45) | collective-permute-done | bytes 393248 | tf_op jit(solution)/shard_map/ppermute | solution.py:462
  172.2 3.8 %collective-permute-start.47 = (bf16[48,2048]{1,0:T(8,128)(2,1)S(1)}, bf16[48,2048]{1,0:T(8,128)(2,1)S(1)}, u32[]{:S(2)}, u32[]{:S(2)}) collective-permute-start(bf16[48,2048]{1,0:T(8,128)(2,1)S(1)} %get-tuple-element.73), channel_id=1, source_target_pairs={{28,0},{24,4},{20,8},{16,12},{12,16},{8,20},{4,24},{0,28},{29,1},{... | collective-permute-start | bytes 589832 | tf_op jit(solution)/shard_map/ppermute | solution.py:477
  176.0 3.3 %collective-permute-done.36 = bf16[96,2048]{1,0:T(8,128)(2,1)S(1)} collective-permute-done((bf16[96,2048]{1,0:T(8,128)(2,1)S(1)}, bf16[96,2048]{1,0:T(8,128)(2,1)S(1)}, u32[]{:S(2)}, u32[]{:S(2)}) %collective-permute-start.36) | collective-permute-done | bytes 393248 | tf_op jit(solution)/shard_map/ppermute | solution.py:462
  179.5 8.2 %collective-permute-done.27 = bf16[96,2048]{1,0:T(8,128)(2,1)S(1)} collective-permute-done((bf16[96,2048]{1,0:T(8,128)(2,1)S(1)}, bf16[96,2048]{1,0:T(8,128)(2,1)S(1)}, u32[]{:S(2)}, u32[]{:S(2)}) %collective-permute-start.27) | collective-permute-done | bytes 393248 | tf_op jit(solution)/shard_map/ppermute | solution.py:462
  187.9 7.8 %collective-permute-done.19 = bf16[96,2048]{1,0:T(8,128)(2,1)S(1)} collective-permute-done((bf16[96,2048]{1,0:T(8,128)(2,1)S(1)}, bf16[96,2048]{1,0:T(8,128)(2,1)S(1)}, u32[]{:S(2)}, u32[]{:S(2)}) %collective-permute-start.19) | collective-permute-done | bytes 393248 | tf_op jit(solution)/shard_map/ppermute | solution.py:462
  195.8 3.1 %collective-permute-start.29 = (bf16[48,2048]{1,0:T(8,128)(2,1)S(1)}, bf16[48,2048]{1,0:T(8,128)(2,1)S(1)}, u32[]{:S(2)}, u32[]{:S(2)}) collective-permute-start(bf16[48,2048]{1,0:T(8,128)(2,1)S(1)} %get-tuple-element.77), channel_id=1, source_target_pairs={{12,0},{8,4},{4,8},{0,12},{28,16},{24,20},{20,24},{16,28},{13,1},{... | collective-permute-start | bytes 589832 | tf_op jit(solution)/shard_map/ppermute | solution.py:477
  199.5 3.1 %collective-permute-done.37.refs_4_ = bf16[48,2048]{1,0:T(8,128)(2,1)S(1)} collective-permute-done((bf16[48,2048]{1,0:T(8,128)(2,1)S(1)}, bf16[48,2048]{1,0:T(8,128)(2,1)S(1)}, u32[]{:S(2)}, u32[]{:S(2)}) %collective-permute-start.37) | collective-permute-done | bytes 196640 | tf_op jit(solution)/shard_map/ppermute | solution.py:477
  202.6 1.9 collective-permute-done.38.refs_5_
  204.5 4.7 %collective-permute-done.28.refs_2_ = bf16[48,2048]{1,0:T(8,128)(2,1)S(1)} collective-permute-done((bf16[48,2048]{1,0:T(8,128)(2,1)S(1)}, bf16[48,2048]{1,0:T(8,128)(2,1)S(1)}, u32[]{:S(2)}, u32[]{:S(2)}) %collective-permute-start.28) | collective-permute-done | bytes 196640 | tf_op jit(solution)/shard_map/ppermute | solution.py:477
  209.2 3.5 %collective-permute-done.29.refs_3_ = bf16[48,2048]{1,0:T(8,128)(2,1)S(1)} collective-permute-done((bf16[48,2048]{1,0:T(8,128)(2,1)S(1)}, bf16[48,2048]{1,0:T(8,128)(2,1)S(1)}, u32[]{:S(2)}, u32[]{:S(2)}) %collective-permute-start.29) | collective-permute-done | bytes 196640 | tf_op jit(solution)/shard_map/ppermute | solution.py:477
  212.8 2.1 combine.1
  (113 shorter events, 20.3 us)
Async XLA Ops:
  3.5 37.2 %all-to-all-start = ((bf16[8,128,384]{2,1,0:T(8,128)(2,1)}), bf16[8,128,384]{2,1,0:T(8,128)(2,1)S(1)}, u32[]{:S(2)}, u32[]{:S(2)}) async-start(bf16[8,128,384]{2,1,0:T(8,128)(2,1)} %get-tuple-element.39), calls=%async_computation | async-start | bytes 1572864 | tf_op jit(solution)/shard_map/all_to_all | solution.py:303
  10.8 9.8 %collective-permute-start = (bf16[128,384]{1,0:T(8,128)(2,1)S(1)}, bf16[128,384]{1,0:T(8,128)(2,1)S(1)}, u32[]{:S(2)}, u32[]{:S(2)}) collective-permute-start(bf16[128,384]{1,0:T(8,128)(2,1)S(1)} %get-tuple-element.41), channel_id=1, source_target_pairs={{0,4},{4,0},{8,12},{12,8},{16,20},{20,16},{24,28},{28,24},{1,5},{5... | collective-permute-start | bytes 294920 | tf_op jit(solution)/shard_map/ppermute | solution.py:308
  12.8 14.0 %collective-permute-start.1 = (bf16[128,384]{1,0:T(8,128)(2,1)S(1)}, bf16[128,384]{1,0:T(8,128)(2,1)S(1)}, u32[]{:S(2)}, u32[]{:S(2)}) collective-permute-start(bf16[128,384]{1,0:T(8,128)(2,1)S(1)} %get-tuple-element.42), channel_id=1, source_target_pairs={{0,8},{4,12},{8,0},{12,4},{16,24},{20,28},{24,16},{28,20},{1,9},{5... | collective-permute-start | bytes 294920 | tf_op jit(solution)/shard_map/ppermute | solution.py:308
  14.3 35.7 %collective-permute-start.2 = (bf16[128,384]{1,0:T(8,128)(2,1)S(1)}, bf16[128,384]{1,0:T(8,128)(2,1)S(1)}, u32[]{:S(2)}, u32[]{:S(2)}) collective-permute-start(bf16[128,384]{1,0:T(8,128)(2,1)S(1)} %get-tuple-element.43), channel_id=1, source_target_pairs={{0,12},{4,8},{8,4},{12,0},{16,28},{20,24},{24,20},{28,16},{1,13},{... | collective-permute-start | bytes 294920 | tf_op jit(solution)/shard_map/ppermute | solution.py:308
  14.3 35.7 %collective-permute-start.3 = (bf16[128,384]{1,0:T(8,128)(2,1)S(1)}, bf16[128,384]{1,0:T(8,128)(2,1)S(1)}, u32[]{:S(2)}, u32[]{:S(2)}) collective-permute-start(bf16[128,384]{1,0:T(8,128)(2,1)S(1)} %get-tuple-element.44), channel_id=1, source_target_pairs={{0,16},{4,20},{8,24},{12,28},{16,0},{20,4},{24,8},{28,12},{1,17},{... | collective-permute-start | bytes 294920 | tf_op jit(solution)/shard_map/ppermute | solution.py:308
  17.2 32.8 %collective-permute-start.4 = (bf16[128,384]{1,0:T(8,128)(2,1)S(1)}, bf16[128,384]{1,0:T(8,128)(2,1)S(1)}, u32[]{:S(2)}, u32[]{:S(2)}) collective-permute-start(bf16[128,384]{1,0:T(8,128)(2,1)S(1)} %get-tuple-element.45), channel_id=1, source_target_pairs={{0,20},{4,16},{8,28},{12,24},{16,4},{20,0},{24,12},{28,8},{1,21},{... | collective-permute-start | bytes 294920 | tf_op jit(solution)/shard_map/ppermute | solution.py:308
  20.6 29.4 %collective-permute-start.5 = (bf16[128,384]{1,0:T(8,128)(2,1)S(1)}, bf16[128,384]{1,0:T(8,128)(2,1)S(1)}, u32[]{:S(2)}, u32[]{:S(2)}) collective-permute-start(bf16[128,384]{1,0:T(8,128)(2,1)S(1)} %get-tuple-element.46), channel_id=1, source_target_pairs={{0,24},{4,28},{8,16},{12,20},{16,8},{20,12},{24,0},{28,4},{1,25},{... | collective-permute-start | bytes 294920 | tf_op jit(solution)/shard_map/ppermute | solution.py:308
  26.9 23.2 %collective-permute-start.6 = (bf16[128,384]{1,0:T(8,128)(2,1)S(1)}, bf16[128,384]{1,0:T(8,128)(2,1)S(1)}, u32[]{:S(2)}, u32[]{:S(2)}) collective-permute-start(bf16[128,384]{1,0:T(8,128)(2,1)S(1)} %get-tuple-element.47), channel_id=1, source_target_pairs={{0,28},{4,24},{8,20},{12,16},{16,12},{20,8},{24,4},{28,0},{1,29},{... | collective-permute-start | bytes 294920 | tf_op jit(solution)/shard_map/ppermute | solution.py:308
  46.6 25.8 %all-to-all-start.1 = ((bf16[8,128,128]{2,1,0:T(8,128)(2,1)}), bf16[8,128,128]{2,1,0:T(8,128)(2,1)S(1)}, u32[]{:S(2)}, u32[]{:S(2)}) async-start(bf16[8,128,128]{2,1,0:T(8,128)(2,1)} %shard_map.145), calls=%async_computation.1 | async-start | bytes 524288 | tf_op jit(solution)/shard_map/all_to_all | solution.py:370
  53.8 9.8 %collective-permute-start.10 = (bf16[128,128]{1,0:T(8,128)(2,1)S(1)}, bf16[128,128]{1,0:T(8,128)(2,1)S(1)}, u32[]{:S(2)}, u32[]{:S(2)}) collective-permute-start(bf16[128,128]{1,0:T(8,128)(2,1)S(1)} %get-tuple-element.52), channel_id=1, source_target_pairs={{16,0},{20,4},{24,8},{28,12},{0,16},{4,20},{8,24},{12,28},{17,1},{... | collective-permute-start | bytes 98312 | tf_op jit(solution)/shard_map/ppermute | solution.py:338
  56.7 6.9 %collective-permute-start.11 = (bf16[128,128]{1,0:T(8,128)(2,1)S(1)}, bf16[128,128]{1,0:T(8,128)(2,1)S(1)}, u32[]{:S(2)}, u32[]{:S(2)}) collective-permute-start(bf16[128,128]{1,0:T(8,128)(2,1)S(1)} %get-tuple-element.53), channel_id=1, source_target_pairs={{20,0},{16,4},{28,8},{24,12},{4,16},{0,20},{12,24},{8,28},{21,1},{... | collective-permute-start | bytes 98312 | tf_op jit(solution)/shard_map/ppermute | solution.py:338
  58.3 7.0 %collective-permute-start.12 = (bf16[128,128]{1,0:T(8,128)(2,1)S(1)}, bf16[128,128]{1,0:T(8,128)(2,1)S(1)}, u32[]{:S(2)}, u32[]{:S(2)}) collective-permute-start(bf16[128,128]{1,0:T(8,128)(2,1)S(1)} %get-tuple-element.54), channel_id=1, source_target_pairs={{24,0},{28,4},{16,8},{20,12},{8,16},{12,20},{0,24},{4,28},{25,1},{... | collective-permute-start | bytes 98312 | tf_op jit(solution)/shard_map/ppermute | solution.py:338
  61.6 6.6 %collective-permute-start.13 = (bf16[128,128]{1,0:T(8,128)(2,1)S(1)}, bf16[128,128]{1,0:T(8,128)(2,1)S(1)}, u32[]{:S(2)}, u32[]{:S(2)}) collective-permute-start(bf16[128,128]{1,0:T(8,128)(2,1)S(1)} %get-tuple-element.55), channel_id=1, source_target_pairs={{28,0},{24,4},{20,8},{16,12},{12,16},{8,20},{4,24},{0,28},{29,1},{... | collective-permute-start | bytes 98312 | tf_op jit(solution)/shard_map/ppermute | solution.py:338
  61.7 6.5 %collective-permute-start.7 = (bf16[128,128]{1,0:T(8,128)(2,1)S(1)}, bf16[128,128]{1,0:T(8,128)(2,1)S(1)}, u32[]{:S(2)}, u32[]{:S(2)}) collective-permute-start(bf16[128,128]{1,0:T(8,128)(2,1)S(1)} %get-tuple-element.49), channel_id=1, source_target_pairs={{4,0},{0,4},{12,8},{8,12},{20,16},{16,20},{28,24},{24,28},{5,1},{1... | collective-permute-start | bytes 98312 | tf_op jit(solution)/shard_map/ppermute | solution.py:338
  63.6 5.0 %collective-permute-start.9 = (bf16[128,128]{1,0:T(8,128)(2,1)S(1)}, bf16[128,128]{1,0:T(8,128)(2,1)S(1)}, u32[]{:S(2)}, u32[]{:S(2)}) collective-permute-start(bf16[128,128]{1,0:T(8,128)(2,1)S(1)} %get-tuple-element.51), channel_id=1, source_target_pairs={{12,0},{8,4},{4,8},{0,12},{28,16},{24,20},{20,24},{16,28},{13,1},{... | collective-permute-start | bytes 98312 | tf_op jit(solution)/shard_map/ppermute | solution.py:338
  78.3 10.5 %collective-permute-start.39 = (bf16[48,2048]{1,0:T(8,128)(2,1)S(1)}, bf16[48,2048]{1,0:T(8,128)(2,1)S(1)}, u32[]{:S(2)}, u32[]{:S(2)}) collective-permute-start(bf16[48,2048]{1,0:T(8,128)(2,1)S(1)} %get-tuple-element.68), channel_id=1, source_target_pairs={{0,28},{4,24},{8,20},{12,16},{16,12},{20,8},{24,4},{28,0},{1,29},{... | collective-permute-start | bytes 589832 | tf_op jit(solution)/shard_map/ppermute | solution.py:470
  81.9 18.0 %collective-permute-start.40 = (bf16[48,2048]{1,0:T(8,128)(2,1)S(1)}, bf16[48,2048]{1,0:T(8,128)(2,1)S(1)}, u32[]{:S(2)}, u32[]{:S(2)}) collective-permute-start(bf16[48,2048]{1,0:T(8,128)(2,1)S(1)} %get-tuple-element.69), channel_id=1, source_target_pairs={{0,24},{4,28},{8,16},{12,20},{16,8},{20,12},{24,0},{28,4},{1,25},{... | collective-permute-start | bytes 589832 | tf_op jit(solution)/shard_map/ppermute | solution.py:470
  82.5 25.3 %collective-permute-start.30 = (bf16[48,2048]{1,0:T(8,128)(2,1)S(1)}, bf16[48,2048]{1,0:T(8,128)(2,1)S(1)}, u32[]{:S(2)}, u32[]{:S(2)}) collective-permute-start(bf16[48,2048]{1,0:T(8,128)(2,1)S(1)} %get-tuple-element.64), channel_id=1, source_target_pairs={{0,20},{4,16},{8,28},{12,24},{16,4},{20,0},{24,12},{28,8},{1,21},{... | collective-permute-start | bytes 589832 | tf_op jit(solution)/shard_map/ppermute | solution.py:470
  85.0 26.0 %collective-permute-start.31 = (bf16[48,2048]{1,0:T(8,128)(2,1)S(1)}, bf16[48,2048]{1,0:T(8,128)(2,1)S(1)}, u32[]{:S(2)}, u32[]{:S(2)}) collective-permute-start(bf16[48,2048]{1,0:T(8,128)(2,1)S(1)} %get-tuple-element.65), channel_id=1, source_target_pairs={{0,16},{4,20},{8,24},{12,28},{16,0},{20,4},{24,8},{28,12},{1,17},{... | collective-permute-start | bytes 589832 | tf_op jit(solution)/shard_map/ppermute | solution.py:470
  86.0 25.0 %collective-permute-start.21 = (bf16[48,2048]{1,0:T(8,128)(2,1)S(1)}, bf16[48,2048]{1,0:T(8,128)(2,1)S(1)}, u32[]{:S(2)}, u32[]{:S(2)}) collective-permute-start(bf16[48,2048]{1,0:T(8,128)(2,1)S(1)} %get-tuple-element.60), channel_id=1, source_target_pairs={{0,12},{4,8},{8,4},{12,0},{16,28},{20,24},{24,20},{28,16},{1,13},{... | collective-permute-start | bytes 589832 | tf_op jit(solution)/shard_map/ppermute | solution.py:470
  88.8 23.8 %collective-permute-start.22 = (bf16[48,2048]{1,0:T(8,128)(2,1)S(1)}, bf16[48,2048]{1,0:T(8,128)(2,1)S(1)}, u32[]{:S(2)}, u32[]{:S(2)}) collective-permute-start(bf16[48,2048]{1,0:T(8,128)(2,1)S(1)} %get-tuple-element.61), channel_id=1, source_target_pairs={{0,8},{4,12},{8,0},{12,4},{16,24},{20,28},{24,16},{28,20},{1,9},{5... | collective-permute-start | bytes 589832 | tf_op jit(solution)/shard_map/ppermute | solution.py:470
  99.9 19.3 %collective-permute-start.14 = (bf16[48,2048]{1,0:T(8,128)(2,1)S(1)}, bf16[48,2048]{1,0:T(8,128)(2,1)S(1)}, u32[]{:S(2)}, u32[]{:S(2)}) collective-permute-start(bf16[48,2048]{1,0:T(8,128)(2,1)S(1)} %get-tuple-element.57), channel_id=1, source_target_pairs={{0,4},{4,0},{8,12},{12,8},{16,20},{20,16},{24,28},{28,24},{1,5},{5... | collective-permute-start | bytes 589832 | tf_op jit(solution)/shard_map/ppermute | solution.py:470
  107.9 11.3 %collective-permute-start.41 = (bf16[96,2048]{1,0:T(8,128)(2,1)S(1)}, bf16[96,2048]{1,0:T(8,128)(2,1)S(1)}, u32[]{:S(2)}, u32[]{:S(2)}) collective-permute-start(bf16[96,2048]{1,0:T(8,128)(2,1)S(1)} %constant_dynamic-update-slice_fusion.6.refs_0_), channel_id=1, source_target_pairs={{0,2},{1,3},{2,0},{3,1},{4,6},{5,7},{6,4},{7,5},{8,10},{9,11},{10,... | collective-permute-start | bytes 1179656 | tf_op jit(solution)/shard_map/ppermute | solution.py:436
  111.0 9.6 %collective-permute-start.42 = (bf16[96,2048]{1,0:T(8,128)(2,1)S(1)}, bf16[96,2048]{1,0:T(8,128)(2,1)S(1)}, u32[]{:S(2)}, u32[]{:S(2)}) collective-permute-start(bf16[96,2048]{1,0:T(8,128)(2,1)S(1)} %constant_dynamic-update-slice_fusion.6.refs_0_), channel_id=1, source_target_pairs={{0,1},{1,0},{2,3},{3,2},{4,5},{5,4},{6,7},{7,6},{8,9},{9,8},{10,11... | collective-permute-start | bytes 1179656 | tf_op jit(solution)/shard_map/ppermute | solution.py:439
  111.0 16.5 %collective-permute-start.32 = (bf16[96,2048]{1,0:T(8,128)(2,1)S(1)}, bf16[96,2048]{1,0:T(8,128)(2,1)S(1)}, u32[]{:S(2)}, u32[]{:S(2)}) collective-permute-start(bf16[96,2048]{1,0:T(8,128)(2,1)S(1)} %constant_dynamic-update-slice_fusion.4.refs_0_), channel_id=1, source_target_pairs={{0,2},{1,3},{2,0},{3,1},{4,6},{5,7},{6,4},{7,5},{8,10},{9,11},{10,... | collective-permute-start | bytes 1179656 | tf_op jit(solution)/shard_map/ppermute | solution.py:436
  112.7 21.4 %collective-permute-start.33 = (bf16[96,2048]{1,0:T(8,128)(2,1)S(1)}, bf16[96,2048]{1,0:T(8,128)(2,1)S(1)}, u32[]{:S(2)}, u32[]{:S(2)}) collective-permute-start(bf16[96,2048]{1,0:T(8,128)(2,1)S(1)} %constant_dynamic-update-slice_fusion.4.refs_0_), channel_id=1, source_target_pairs={{0,1},{1,0},{2,3},{3,2},{4,5},{5,4},{6,7},{7,6},{8,9},{9,8},{10,11... | collective-permute-start | bytes 1179656 | tf_op jit(solution)/shard_map/ppermute | solution.py:439
  119.1 9.8 %collective-permute-start.43 = (bf16[96,2048]{1,0:T(8,128)(2,1)S(1)}, bf16[96,2048]{1,0:T(8,128)(2,1)S(1)}, u32[]{:S(2)}, u32[]{:S(2)}) collective-permute-start(bf16[96,2048]{1,0:T(8,128)(2,1)S(1)} %collective-permute-done.41.refs_1_), channel_id=1, source_target_pairs={{0,1},{1,0},{2,3},{3,2},{4,5},{5,4},{6,7},{7,6},{8,9},{9,8},{10,11... | collective-permute-start | bytes 1179656 | tf_op jit(solution)/shard_map/ppermute | solution.py:439
  119.2 16.8 %collective-permute-start.23 = (bf16[96,2048]{1,0:T(8,128)(2,1)S(1)}, bf16[96,2048]{1,0:T(8,128)(2,1)S(1)}, u32[]{:S(2)}, u32[]{:S(2)}) collective-permute-start(bf16[96,2048]{1,0:T(8,128)(2,1)S(1)} %constant_dynamic-update-slice_fusion.2.refs_0_), channel_id=1, source_target_pairs={{0,2},{1,3},{2,0},{3,1},{4,6},{5,7},{6,4},{7,5},{8,10},{9,11},{10,... | collective-permute-start | bytes 1179656 | tf_op jit(solution)/shard_map/ppermute | solution.py:436
  120.7 26.9 %collective-permute-start.24 = (bf16[96,2048]{1,0:T(8,128)(2,1)S(1)}, bf16[96,2048]{1,0:T(8,128)(2,1)S(1)}, u32[]{:S(2)}, u32[]{:S(2)}) collective-permute-start(bf16[96,2048]{1,0:T(8,128)(2,1)S(1)} %constant_dynamic-update-slice_fusion.2.refs_0_), channel_id=1, source_target_pairs={{0,1},{1,0},{2,3},{3,2},{4,5},{5,4},{6,7},{7,6},{8,9},{9,8},{10,11... | collective-permute-start | bytes 1179656 | tf_op jit(solution)/shard_map/ppermute | solution.py:439
  127.6 14.4 %collective-permute-start.15 = (bf16[96,2048]{1,0:T(8,128)(2,1)S(1)}, bf16[96,2048]{1,0:T(8,128)(2,1)S(1)}, u32[]{:S(2)}, u32[]{:S(2)}) collective-permute-start(bf16[96,2048]{1,0:T(8,128)(2,1)S(1)} %constant_dynamic-update-slice_fusion.refs_0_), channel_id=1, source_target_pairs={{0,2},{1,3},{2,0},{3,1},{4,6},{5,7},{6,4},{7,5},{8,10},{9,11},{10,... | collective-permute-start | bytes 1179656 | tf_op jit(solution)/shard_map/ppermute | solution.py:436
  129.0 13.0 %collective-permute-start.34 = (bf16[96,2048]{1,0:T(8,128)(2,1)S(1)}, bf16[96,2048]{1,0:T(8,128)(2,1)S(1)}, u32[]{:S(2)}, u32[]{:S(2)}) collective-permute-start(bf16[96,2048]{1,0:T(8,128)(2,1)S(1)} %collective-permute-done.32.refs_1_), channel_id=1, source_target_pairs={{0,1},{1,0},{2,3},{3,2},{4,5},{5,4},{6,7},{7,6},{8,9},{9,8},{10,11... | collective-permute-start | bytes 1179656 | tf_op jit(solution)/shard_map/ppermute | solution.py:439
  134.1 19.4 %collective-permute-start.16 = (bf16[96,2048]{1,0:T(8,128)(2,1)S(1)}, bf16[96,2048]{1,0:T(8,128)(2,1)S(1)}, u32[]{:S(2)}, u32[]{:S(2)}) collective-permute-start(bf16[96,2048]{1,0:T(8,128)(2,1)S(1)} %constant_dynamic-update-slice_fusion.refs_0_), channel_id=1, source_target_pairs={{0,1},{1,0},{2,3},{3,2},{4,5},{5,4},{6,7},{7,6},{8,9},{9,8},{10,11... | collective-permute-start | bytes 1179656 | tf_op jit(solution)/shard_map/ppermute | solution.py:439
  136.0 11.6 %collective-permute-start.25 = (bf16[96,2048]{1,0:T(8,128)(2,1)S(1)}, bf16[96,2048]{1,0:T(8,128)(2,1)S(1)}, u32[]{:S(2)}, u32[]{:S(2)}) collective-permute-start(bf16[96,2048]{1,0:T(8,128)(2,1)S(1)} %collective-permute-done.23.refs_1_), channel_id=1, source_target_pairs={{0,1},{1,0},{2,3},{3,2},{4,5},{5,4},{6,7},{7,6},{8,9},{9,8},{10,11... | collective-permute-start | bytes 1179656 | tf_op jit(solution)/shard_map/ppermute | solution.py:439
  141.9 11.6 %collective-permute-start.17 = (bf16[96,2048]{1,0:T(8,128)(2,1)S(1)}, bf16[96,2048]{1,0:T(8,128)(2,1)S(1)}, u32[]{:S(2)}, u32[]{:S(2)}) collective-permute-start(bf16[96,2048]{1,0:T(8,128)(2,1)S(1)} %collective-permute-done.15.refs_1_), channel_id=1, source_target_pairs={{0,1},{1,0},{2,3},{3,2},{4,5},{5,4},{6,7},{7,6},{8,9},{9,8},{10,11... | collective-permute-start | bytes 1179656 | tf_op jit(solution)/shard_map/ppermute | solution.py:439
  142.0 16.7 %collective-permute-start.44 = (bf16[2,96,2048]{2,1,0:T(8,128)(2,1)S(1)}, bf16[2,96,2048]{2,1,0:T(8,128)(2,1)S(1)}, u32[]{:S(2)}, u32[]{:S(2)}) collective-permute-start(bf16[2,96,2048]{2,1,0:T(8,128)(2,1)S(1)} %get-tuple-element.71), channel_id=1, source_target_pairs={{0,1},{1,0},{2,3},{3,2},{4,5},{5,4},{6,7},{7,6},{8,9},{9,8},{10,11... | collective-permute-start | bytes 2359304 | tf_op jit(solution)/shard_map/ppermute | solution.py:458
  147.5 12.8 %collective-permute-start.35 = (bf16[2,96,2048]{2,1,0:T(8,128)(2,1)S(1)}, bf16[2,96,2048]{2,1,0:T(8,128)(2,1)S(1)}, u32[]{:S(2)}, u32[]{:S(2)}) collective-permute-start(bf16[2,96,2048]{2,1,0:T(8,128)(2,1)S(1)} %get-tuple-element.67), channel_id=1, source_target_pairs={{0,1},{1,0},{2,3},{3,2},{4,5},{5,4},{6,7},{7,6},{8,9},{9,8},{10,11... | collective-permute-start | bytes 2359304 | tf_op jit(solution)/shard_map/ppermute | solution.py:458
  152.9 8.1 %collective-permute-start.26 = (bf16[2,96,2048]{2,1,0:T(8,128)(2,1)S(1)}, bf16[2,96,2048]{2,1,0:T(8,128)(2,1)S(1)}, u32[]{:S(2)}, u32[]{:S(2)}) collective-permute-start(bf16[2,96,2048]{2,1,0:T(8,128)(2,1)S(1)} %get-tuple-element.63), channel_id=1, source_target_pairs={{0,1},{1,0},{2,3},{3,2},{4,5},{5,4},{6,7},{7,6},{8,9},{9,8},{10,11... | collective-permute-start | bytes 2359304 | tf_op jit(solution)/shard_map/ppermute | solution.py:458
  158.8 12.1 %collective-permute-start.45 = (bf16[96,2048]{1,0:T(8,128)(2,1)S(1)}, bf16[96,2048]{1,0:T(8,128)(2,1)S(1)}, u32[]{:S(2)}, u32[]{:S(2)}) collective-permute-start(bf16[96,2048]{1,0:T(8,128)(2,1)S(1)} %fusion.7), channel_id=1, source_target_pairs={{0,2},{1,3},{2,0},{3,1},{4,6},{5,7},{6,4},{7,5},{8,10},{9,11},{10,... | collective-permute-start | bytes 1179656 | tf_op jit(solution)/shard_map/ppermute | solution.py:462
  160.4 18.8 %collective-permute-start.36 = (bf16[96,2048]{1,0:T(8,128)(2,1)S(1)}, bf16[96,2048]{1,0:T(8,128)(2,1)S(1)}, u32[]{:S(2)}, u32[]{:S(2)}) collective-permute-start(bf16[96,2048]{1,0:T(8,128)(2,1)S(1)} %fusion.6), channel_id=1, source_target_pairs={{0,2},{1,3},{2,0},{3,1},{4,6},{5,7},{6,4},{7,5},{8,10},{9,11},{10,... | collective-permute-start | bytes 1179656 | tf_op jit(solution)/shard_map/ppermute | solution.py:462
  161.2 26.5 %collective-permute-start.27 = (bf16[96,2048]{1,0:T(8,128)(2,1)S(1)}, bf16[96,2048]{1,0:T(8,128)(2,1)S(1)}, u32[]{:S(2)}, u32[]{:S(2)}) collective-permute-start(bf16[96,2048]{1,0:T(8,128)(2,1)S(1)} %fusion.5), channel_id=1, source_target_pairs={{0,2},{1,3},{2,0},{3,1},{4,6},{5,7},{6,4},{7,5},{8,10},{9,11},{10,... | collective-permute-start | bytes 1179656 | tf_op jit(solution)/shard_map/ppermute | solution.py:462
  162.8 32.8 %collective-permute-start.19 = (bf16[96,2048]{1,0:T(8,128)(2,1)S(1)}, bf16[96,2048]{1,0:T(8,128)(2,1)S(1)}, u32[]{:S(2)}, u32[]{:S(2)}) collective-permute-start(bf16[96,2048]{1,0:T(8,128)(2,1)S(1)} %fusion.4), channel_id=1, source_target_pairs={{0,2},{1,3},{2,0},{3,1},{4,6},{5,7},{6,4},{7,5},{8,10},{9,11},{10,... | collective-permute-start | bytes 1179656 | tf_op jit(solution)/shard_map/ppermute | solution.py:462
  171.0 24.8 %collective-permute-start.46 = (bf16[48,2048]{1,0:T(8,128)(2,1)S(1)}, bf16[48,2048]{1,0:T(8,128)(2,1)S(1)}, u32[]{:S(2)}, u32[]{:S(2)}) collective-permute-start(bf16[48,2048]{1,0:T(8,128)(2,1)S(1)} %get-tuple-element.74), channel_id=1, source_target_pairs={{24,0},{28,4},{16,8},{20,12},{8,16},{12,20},{0,24},{4,28},{25,1},{... | collective-permute-start | bytes 589832 | tf_op jit(solution)/shard_map/ppermute | solution.py:477
  172.2 26.7 %collective-permute-start.47 = (bf16[48,2048]{1,0:T(8,128)(2,1)S(1)}, bf16[48,2048]{1,0:T(8,128)(2,1)S(1)}, u32[]{:S(2)}, u32[]{:S(2)}) collective-permute-start(bf16[48,2048]{1,0:T(8,128)(2,1)S(1)} %get-tuple-element.73), channel_id=1, source_target_pairs={{28,0},{24,4},{20,8},{16,12},{12,16},{8,20},{4,24},{0,28},{29,1},{... | collective-permute-start | bytes 589832 | tf_op jit(solution)/shard_map/ppermute | solution.py:477
  179.4 23.2 %collective-permute-start.37 = (bf16[48,2048]{1,0:T(8,128)(2,1)S(1)}, bf16[48,2048]{1,0:T(8,128)(2,1)S(1)}, u32[]{:S(2)}, u32[]{:S(2)}) collective-permute-start(bf16[48,2048]{1,0:T(8,128)(2,1)S(1)} %get-tuple-element.76), channel_id=1, source_target_pairs={{16,0},{20,4},{24,8},{28,12},{0,16},{4,20},{8,24},{12,28},{17,1},{... | collective-permute-start | bytes 589832 | tf_op jit(solution)/shard_map/ppermute | solution.py:477
  187.7 16.8 %collective-permute-start.38 = (bf16[48,2048]{1,0:T(8,128)(2,1)S(1)}, bf16[48,2048]{1,0:T(8,128)(2,1)S(1)}, u32[]{:S(2)}, u32[]{:S(2)}) collective-permute-start(bf16[48,2048]{1,0:T(8,128)(2,1)S(1)} %get-tuple-element.75), channel_id=1, source_target_pairs={{20,0},{16,4},{28,8},{24,12},{4,16},{0,20},{12,24},{8,28},{21,1},{... | collective-permute-start | bytes 589832 | tf_op jit(solution)/shard_map/ppermute | solution.py:477
  195.6 13.6 %collective-permute-start.28 = (bf16[48,2048]{1,0:T(8,128)(2,1)S(1)}, bf16[48,2048]{1,0:T(8,128)(2,1)S(1)}, u32[]{:S(2)}, u32[]{:S(2)}) collective-permute-start(bf16[48,2048]{1,0:T(8,128)(2,1)S(1)} %get-tuple-element.78), channel_id=1, source_target_pairs={{8,0},{12,4},{0,8},{4,12},{24,16},{28,20},{16,24},{20,28},{9,1},{1... | collective-permute-start | bytes 589832 | tf_op jit(solution)/shard_map/ppermute | solution.py:477
  195.8 16.9 %collective-permute-start.29 = (bf16[48,2048]{1,0:T(8,128)(2,1)S(1)}, bf16[48,2048]{1,0:T(8,128)(2,1)S(1)}, u32[]{:S(2)}, u32[]{:S(2)}) collective-permute-start(bf16[48,2048]{1,0:T(8,128)(2,1)S(1)} %get-tuple-element.77), channel_id=1, source_target_pairs={{12,0},{8,4},{4,8},{0,12},{28,16},{24,20},{20,24},{16,28},{13,1},{... | collective-permute-start | bytes 589832 | tf_op jit(solution)/shard_map/ppermute | solution.py:477
  199.0 13.8 %collective-permute-start.20 = (bf16[48,2048]{1,0:T(8,128)(2,1)S(1)}, bf16[48,2048]{1,0:T(8,128)(2,1)S(1)}, u32[]{:S(2)}, u32[]{:S(2)}) collective-permute-start(bf16[48,2048]{1,0:T(8,128)(2,1)S(1)} %get-tuple-element.79), channel_id=1, source_target_pairs={{4,0},{0,4},{12,8},{8,12},{20,16},{16,20},{28,24},{24,28},{5,1},{1... | collective-permute-start | bytes 589832 | tf_op jit(solution)/shard_map/ppermute | solution.py:477
  (14 other events, 277.4 us)
